TPU v7x, 32 devices: a whole 2x2x4 slice. The times are simulated.
32 devices in a mesh: grp: 2 (over y), ep: 4 (over z), tp: 4 (over x, core).
Axes of the slice: x: 2, y: 2, z: 4, core: 2. Of those that a mesh axis runs over, the one named last changes fastest.
Arguments:
- conv_x: bfloat16 [8192, 2048], P(('grp', 'ep', 'tp')), parts along dimension 0, may hold values from -6 to 6
- conv_c: bfloat16 [8192, 2048], P(('grp', 'ep', 'tp')), parts along dimension 0, may hold values from -6 to 6
- conv_b: bfloat16 [8192, 2048], P(('grp', 'ep', 'tp')), parts along dimension 0, may hold values from -6 to 6
- conv_taps: float32 [3, 2048], replicated, may hold values from -3.5 to 3.5
- w_out: bfloat16 [2048, 2048], P('tp'), may hold values from -0.125 to 0.125
- tokens_b: bfloat16 [4096, 2048], P(('grp', 'ep', 'tp')), parts along dimension 0, may hold values from -6 to 6
- norm_gain: float32 [2048], replicated, may hold values from 0.1 to 1.9
- route_b: int32 [4096, 2], P(('grp', 'ep', 'tp')), parts along dimension 0, may hold values from 0 to 3, all different within a row; in each aligned block of 128 rows (0 to 127, 128 to 255, ...) at most 128 rows name the same one
- route_weights: float32 [4096, 2], P(('grp', 'ep', 'tp')), parts along dimension 0, may hold values from 0.1 to 1
- w_gate: bfloat16 [4, 2048, 1024], P('ep', None, 'tp'), may hold values from -0.125 to 0.125
- w_up: bfloat16 [4, 2048, 1024], P('ep', None, 'tp'), may hold values from -0.125 to 0.125
- w_down: bfloat16 [4, 1024, 2048], P('ep', 'tp'), may hold values from -0.1875 to 0.1875
Outputs:
- mixed_a: bfloat16 [8192, 2048], P(('grp', 'ep', 'tp')), parts along dimension 0
- experts_b: bfloat16 [4096, 2048], P(('grp', 'ep', 'tp')), parts along dimension 0
There are 2 independent parts, one for each index of `grp`. A program takes and returns all parts, laid end to end along the dimension named above; an argument that names none is the same for every part. Nothing has to cross between parts.
Inputs may be any that keep to these rules, and one draw needn't show every extreme that they name: `route_b`: the 2 experts of a row differ. Within the 128 rows of one device no expert is named more than 128 times, and in every draw some device names some expert exactly 128 times.
All inputs are finite; a program needn't handle non-finite values.
Results may differ from a plain program's by a relative error of at most 0.012.
Values may be sent and summed in bfloat16 or wider, within the bound.
No kernel may reach another device: no remote copies, remote signals or barrier semaphores. Data moves between devices by JAX's collectives and lax.ppermute only.
A program may use at most 128 MiB of HBM per device.

v0:
```python
import jax
import jax.numpy as jnp
from jax import lax
from jax.sharding import PartitionSpec as P

D = 2048
TOPK = 2


def shifted(x, axis, by):
    size = lax.axis_size(axis)
    pairs = [(i, i + by) for i in range(size) if 0 <= i + by < size]
    return lax.ppermute(x, axis, pairs)


def slot_targets(route, experts, capacity):
    flat = route.reshape(-1)
    onehot = (flat[:, None] == jnp.arange(experts, dtype=jnp.int32)[None, :]).astype(jnp.int32)
    earlier = jnp.cumsum(onehot, axis=0) - onehot
    ranks = jnp.sum(earlier * onehot, axis=1).reshape(route.shape)
    return route * capacity + ranks


def fill_slots(targets, slot_total, filler):
    token_ids = jnp.repeat(jnp.arange(filler, dtype=jnp.int32), targets.shape[1])
    return jnp.full((slot_total,), filler, jnp.int32).at[targets.reshape(-1)].set(token_ids)


def expert_hidden(rows, weight_gate, weight_up):
    gate_val = jnp.dot(rows, weight_gate, preferred_element_type=jnp.float32)
    up_val = jnp.dot(rows, weight_up, preferred_element_type=jnp.float32)
    return (jax.nn.silu(gate_val) * up_val).astype(jnp.bfloat16)


def per_device(
    conv_x,
    conv_c,
    conv_b,
    conv_taps,
    w_out,
    tokens_b,
    norm_gain,
    route_b,
    route_weights,
    w_gate,
    w_up,
    w_down,
):
    rows_mix = conv_x.shape[0]
    reach_rows = conv_taps.shape[0] - 1
    mixed_u = (conv_c.astype(jnp.float32) * conv_x.astype(jnp.float32)).astype(jnp.bfloat16)
    before = shifted(mixed_u[rows_mix - reach_rows :], ("ep", "tp"), 1)
    extended = jnp.concatenate([before, mixed_u], axis=0)
    filtered = jnp.zeros(mixed_u.shape, jnp.float32)
    for shift_tap in range(reach_rows + 1):
        filtered = filtered + conv_taps[shift_tap][None, :] * extended[
            shift_tap : shift_tap + rows_mix
        ].astype(jnp.float32)
    gated_rows = (conv_b.astype(jnp.float32) * filtered).astype(jnp.bfloat16)
    mixed_out = jnp.dot(
        gated_rows,
        lax.all_gather(w_out, "tp", axis=0, tiled=True),
        preferred_element_type=jnp.float32,
    )
    mixed_a = mixed_out.astype(jnp.bfloat16)
    tokens_f = tokens_b.astype(jnp.float32)
    normed = (
        tokens_f
        * lax.rsqrt(jnp.mean(tokens_f * tokens_f, axis=-1, keepdims=True) + 1e-06)
        * norm_gain
    ).astype(jnp.bfloat16)
    experts = lax.axis_size("ep")
    rows_exp = route_b.shape[0]
    capacity = 2 * rows_exp * TOPK // experts
    slot_total = experts * capacity
    targets = slot_targets(route_b, experts, capacity)
    weight_gate = w_gate[0]
    weight_up = w_up[0]
    weight_down = w_down[0]
    padded_rows = jnp.concatenate([normed, jnp.zeros((1, D), jnp.bfloat16)], axis=0)
    outgoing = padded_rows[fill_slots(targets, slot_total, rows_exp)]
    arrived = lax.all_to_all(outgoing, "ep", split_axis=0, concat_axis=0, tiled=True)
    hidden = expert_hidden(
        lax.all_gather(arrived, "tp", axis=0, tiled=True), weight_gate, weight_up
    )
    summed = lax.psum_scatter(
        jnp.dot(hidden, weight_down, preferred_element_type=jnp.float32).astype(jnp.bfloat16),
        "tp",
        scatter_dimension=0,
        tiled=True,
    )
    returned = lax.all_to_all(summed, "ep", split_axis=0, concat_axis=0, tiled=True)
    picked = returned[targets]
    shares = route_weights / jnp.sum(route_weights, axis=-1, keepdims=True)
    experts_b = jnp.sum(picked.astype(jnp.float32) * shares[:, :, None], axis=1).astype(
        jnp.bfloat16
    )
    return (mixed_a, experts_b)


def solution(mesh):
    return jax.shard_map(
        per_device,
        mesh=mesh,
        in_specs=(
            P(("grp", "ep", "tp"), None),
            P(("grp", "ep", "tp"), None),
            P(("grp", "ep", "tp"), None),
            P(),
            P("tp", None),
            P(("grp", "ep", "tp"), None),
            P(),
            P(("grp", "ep", "tp"), None),
            P(("grp", "ep", "tp"), None),
            P("ep", None, "tp"),
            P("ep", None, "tp"),
            P("ep", "tp", None),
        ),
        out_specs=(P(("grp", "ep", "tp"), None), P(("grp", "ep", "tp"), None)),
        check_vma=False,
    )
```

profile of v0, /device:TPU:0, one launch (start us, length us, event | category | flops | bytes accessed | tf_op | source)
XLA Modules:
  0.0 306.5 jit_solution(13236380479870054921)
XLA Ops:
  7.2 0.9 copy.24
  8.1 0.1 eq.29
  8.2 0.1 eq.25
  8.4 1.2 reduce-window.6
  10.0 0.1 reshape.74
  10.2 0.7 compare_select_fusion.2
  10.9 0.1 copy.29
  11.1 0.1 reshape.75
  11.2 0.1 reshape.97
  11.4 1.4 scatter_custom_fusion
  12.8 1.2 fusion.2
  14.0 1.2 fusion.4
  15.3 3.3 %gather_fusion = bf16[512,2048]{1,0:T(8,128)(2,1)} fusion(bf16[129,2048]{1,0:T(8,128)(2,1)S(1)} %concatenate.7, s32[1024]{0:T(1024)S(1)} %pad_clamp_fusion.1), kind=kCustom, calls=%fused_computation | custom fusion | bytes 4196352 | tf_op jit(solution)/shard_map/gather | solution.py:81
  18.6 54.6 %all_to_all.24 = bf16[4,128,2048]{2,1,0:T(8,128)(2,1)} all-to-all(bf16[4,128,2048]{2,1,0:T(8,128)(2,1)} %bitcast.41), channel_id=1, replica_groups=mesh['grp'=2,'ep'=4,'tp'=4] {'ep'}, dimensions={0} | all-to-all | bytes 4194304 | tf_op jit(solution)/shard_map/all_to_all | solution.py:82
  73.4 57.6 %all-gather.5.cloned.1.call-done = bf16[2048,2048]{1,0:T(8,128)(2,1)} async-done(((bf16[512,2048]{1,0:T(8,128)(2,1)}), bf16[2048,2048]{1,0:T(8,128)(2,1)}) %all-gather.5.cloned.1.call-update) | async-done | bytes 8388624 | tf_op jit(solution)/shard_map/all_gather | solution.py:84
  130.9 7.1 %fusion.9 = f32[2048,256]{1,0:T(8,128)} fusion(bf16[2048,2048]{1,0:T(8,128)(2,1)} %all-gather.5.cloned.1.call-done, bf16[1,2048,256]{2,1,0:T(8,128)(2,1)S(1)} %copy-done.4), kind=kOutput, calls=%fused_computation.22 | convolution fusion | flops 2147483648 | bytes 11534336 | tf_op jit(solution)/shard_map/dot_general | solution.py:30
  138.0 13.2 %convolution_convert_fusion = bf16[2048,2048]{1,0:T(8,128)(2,1)} fusion(bf16[2048,2048]{1,0:T(8,128)(2,1)} %all-gather.5.cloned.1.call-done, f32[2048,256]{1,0:T(8,128)} %fusion.9, bf16[1,256,2048]{2,1,0:T(8,128)(2,1)S(1)} %copy-done, bf16[1,2048,256]{2,1,0:T(8,128)(2,1)S(1)} %copy-done.5), kind=kOutput, calls=%fused_computation.3 | convolution fusion | flops 4302307328 | bytes 20971520 | tf_op jit(solution)/shard_map/dot_general | solution.py:87
  151.3 0.7 all-gather.3.cloned.1.call-update
  152.0 70.8 %reduce-scatter.2.cloned.1.call-done = bf16[512,2048]{1,0:T(8,128)(2,1)} async-done(((bf16[2048,2048]{1,0:T(8,128)(2,1)}), bf16[512,2048]{1,0:T(8,128)(2,1)}) %reduce-scatter.2.cloned.1.call-update) | async-done | bytes 2097168 | tf_op jit(solution)/shard_map/reduce_scatter | solution.py:86
  222.8 4.6 %all-to-all-start.1 = ((bf16[4,128,2048]{2,1,0:T(8,128)(2,1)}), bf16[4,128,2048]{2,1,0:T(8,128)(2,1)S(1)}, u32[]{:S(2)}, u32[]{:S(2)}) async-start(bf16[4,128,2048]{2,1,0:T(8,128)(2,1)} %bitcast.43), calls=%async_computation.2 | async-start | bytes 4194304 | tf_op jit(solution)/shard_map/all_to_all | solution.py:92
  227.4 1.9 multiply_convert_fusion.1
  229.3 1.0 copy-done.1
  230.3 1.5 collective-permute-start
  231.8 0.1 copy.30
  232.0 0.1 reshape.87
  232.2 0.1 copy.31
  232.3 0.2 collective-permute-done
  232.5 50.2 %all-gather.3.cloned.1.call-done = bf16[2048,2048]{1,0:T(8,128)(2,1)} async-done(((bf16[512,2048]{1,0:T(8,128)(2,1)}), bf16[2048,2048]{1,0:T(8,128)(2,1)}) %all-gather.3.cloned.1.call-update) | async-done | bytes 8388624 | tf_op jit(solution)/shard_map/all_gather | solution.py:62
  282.7 8.6 %convolution_convert_fusion.1 = bf16[256,2048]{1,0:T(8,128)(2,1)} fusion(bf16[2048,2048]{1,0:T(8,128)(2,1)} %all-gather.3.cloned.1.call-done, bf16[256,2048]{1,0:T(8,128)(2,1)} %copy-done.1, bf16[256,2048]{1,0:T(8,128)(2,1)} %param.14, bf16[2,2048]{1,0:T(2,128)(2,1)S(1)} %collective-permute-done, f32[2048]{0:T(1024)S(1)} %bitcast.45, f32[2048]{0:T(1024)S(1)} %bitcast.46, ...), kind=kOutput, calls=%fused_computation.6 | convolution fusion | flops 2156920832 | bytes 11567104 | tf_op jit(solution)/shard_map/dot_general | solution.py:60
  291.3 2.3 gather_fusion.1
  293.6 2.4 reshape.104
  296.0 3.9 %multiply_reduce_fusion = bf16[128,2048]{1,0:T(8,128)(2,1)} fusion(f32[128,2,2048]{2,1,0:T(2,128)S(1)} %reshape.104, f32[128,2]{1,0:T(8,128)S(1)} %copy.31), kind=kLoop, calls=%fused_computation.7 | loop fusion | flops 786432 | bytes 2622464 | tf_op jit(solution)/shard_map/reduce_sum | solution.py:95
  (37 shorter events, 0.8 us)
Async XLA Ops:
  7.2 130.9 %copy-start = (bf16[1,256,2048]{2,1,0:T(8,128)(2,1)S(1)}, bf16[1,256,2048]{2,1,0:T(8,128)(2,1)}, u32[]{:S(2)}) copy-start(bf16[1,256,2048]{2,1,0:T(8,128)(2,1)} %param.23) | copy-start | bytes 3145732
  7.2 123.8 %all-gather.5.cloned.1.call-start = ((), (), s32[]{:S(2)}) async-start(), calls=%async_computation.4 | async-start | bytes 10485760 | tf_op jit(solution)/shard_map/all_gather | solution.py:84
  73.3 57.7 %copy-start.4 = (bf16[1,2048,256]{2,1,0:T(8,128)(2,1)S(1)}, bf16[1,2048,256]{2,1,0:T(8,128)(2,1)}, u32[]{:S(2)}) copy-start(bf16[1,2048,256]{2,1,0:T(8,128)(2,1)} %param.21) | copy-start | bytes 3145732
  73.3 64.7 %copy-start.5 = (bf16[1,2048,256]{2,1,0:T(8,128)(2,1)S(1)}, bf16[1,2048,256]{2,1,0:T(8,128)(2,1)}, u32[]{:S(2)}) copy-start(bf16[1,2048,256]{2,1,0:T(8,128)(2,1)} %param.22) | copy-start | bytes 3145732
  73.3 149.5 %reduce-scatter.2.cloned.1.call-start = ((), (), s32[]{:S(2)}) async-start(), calls=%async_computation.5 | async-start | bytes 10485760 | tf_op jit(solution)/shard_map/reduce_scatter | solution.py:86
  151.2 131.4 %all-gather.3.cloned.1.call-start = ((), (), s32[]{:S(2)}) async-start(), calls=%async_computation.3 | async-start | bytes 10485760 | tf_op jit(solution)/shard_map/all_gather | solution.py:62
  222.8 68.5 %all-to-all-start.1 = ((bf16[4,128,2048]{2,1,0:T(8,128)(2,1)}), bf16[4,128,2048]{2,1,0:T(8,128)(2,1)S(1)}, u32[]{:S(2)}, u32[]{:S(2)}) async-start(bf16[4,128,2048]{2,1,0:T(8,128)(2,1)} %bitcast.43), calls=%async_computation.2 | async-start | bytes 4194304 | tf_op jit(solution)/shard_map/all_to_all | solution.py:92
  227.4 4.7 %copy-start.3 = (f32[128,2]{0,1:T(2,128)S(1)}, f32[128,2]{0,1:T(2,128)}, u32[]{:S(2)}) copy-start(f32[128,2]{0,1:T(2,128)} %param.20) | copy-start | bytes 3076
  227.4 4.8 %copy-start.2 = (f32[3,2048]{1,0:T(4,128)S(1)}, f32[3,2048]{1,0:T(4,128)}, u32[]{:S(2)}) copy-start(f32[3,2048]{1,0:T(4,128)} %param.15) | copy-start | bytes 73732
  229.3 1.0 copy-start.1
  230.3 2.1 collective-permute-start
Sparse Core Ops, SparseCore 0:
  73.4 57.4 all-gather.4
  151.3 71.3 reduce-scatter.1
  224.3 58.2 all-gather.2
where the time goes:
time: 307 us; the launch traced here: 306 us
  waiting for transfers between devices  179 us (58%)
  blocking collectives  54.6 us (18%)
  matrix products  28.9 us (9%)
  between operations  13.9 us (5%)
  local copies, waits for them, and re-layouts  12.9 us (4%)
  other arithmetic  10.5 us (3%)
  starting transfers between devices  6.22 us (2%)
    reduce_scatter x1, waiting for transfers between devices, per_device(): lax.psum_scatter(jnp.dot(hidden, weight_down, preferred_element_type=jnp....  70.8 us
    all_gather x1, waiting for transfers between devices, per_device(): lax.all_gather(arrived, 'tp', axis=0, tiled=True)  57.6 us
    all_to_all x1, blocking collectives, per_device(): lax.all_to_all(outgoing, 'ep', split_axis=0, concat_axis=0, tiled=True)  54.6 us
    all_gather x1, waiting for transfers between devices, per_device(): lax.all_gather(w_out, 'tp', axis=0, tiled=True)  50.2 us
    dot_general x1, matrix products, per_device(): jnp.dot(hidden, weight_down, preferred_element_type=jnp.float32)  13.2 us
    dot_general x1, matrix products, per_device(): jnp.dot(gated_rows, lax.all_gather(w_out, 'tp', axis=0, tiled=True), pref...  8.61 us
    dot_general x1, matrix products, expert_hidden(): gate_val = jnp.dot(rows, weight_gate, preferred_element_type=jnp.float32)  7.09 us
  transfers between devices with their start and end apart: 5, of which 4 were waited for; matrix products, arithmetic and copies ran while one was open for 4% of the time, Pallas kernels for 0%

commit v1 on v0

--- a/solution.py
+++ b/solution.py
@@ -98,9 +98,145 @@
     return (mixed_a, experts_b)
 
 
+def swapped(x, axis, mask):
+    return lax.ppermute(x, axis, [(i, i ^ mask) for i in range(lax.axis_size(axis))])
+
+
+def turned(x, axis, by):
+    size = lax.axis_size(axis)
+    return lax.ppermute(x, axis, [(i, (i + by) % size) for i in range(size)])
+
+
+def gathered_pieces(w_out):
+    me = lax.axis_index("tp")
+    grp = lax.axis_index("grp")
+    rows = w_out.shape[0]
+    half = rows // 2
+    mine = lax.dynamic_slice_in_dim(w_out, grp * half, half, axis=0)
+    far_mine = swapped(mine, "tp", 2)
+    far_other = swapped(far_mine, "grp", 1)
+    near = swapped(w_out, "tp", 1)
+    diag_mine = swapped(far_mine, "tp", 1)
+    diag_other = swapped(far_other, "tp", 1)
+    return [
+        (me * rows, w_out),
+        ((me ^ 1) * rows, near),
+        ((me ^ 2) * rows + grp * half, far_mine),
+        ((me ^ 3) * rows + grp * half, diag_mine),
+        ((me ^ 2) * rows + (1 - grp) * half, far_other),
+        ((me ^ 3) * rows + (1 - grp) * half, diag_other),
+    ]
+
+
+def dense_per_device(
+    conv_x,
+    conv_c,
+    conv_b,
+    conv_taps,
+    w_out,
+    tokens_b,
+    norm_gain,
+    route_b,
+    route_weights,
+    w_gate,
+    w_up,
+    w_down,
+):
+    n_ep = lax.axis_size("ep")
+    n_tp = lax.axis_size("tp")
+    my_ep = lax.axis_index("ep")
+    my_tp = lax.axis_index("tp")
+    rows_exp = route_b.shape[0]
+    pieces = gathered_pieces(w_out)
+    tokens_f = tokens_b.astype(jnp.float32)
+    normed = (
+        tokens_f
+        * lax.rsqrt(jnp.mean(tokens_f * tokens_f, axis=-1, keepdims=True) + 1e-06)
+        * norm_gain
+    ).astype(jnp.bfloat16)
+    shares = route_weights / jnp.sum(route_weights, axis=-1, keepdims=True)
+    named = route_b[:, :, None] == jnp.arange(n_ep, dtype=jnp.int32)[None, None, :]
+    spread = jnp.sum(jnp.where(named, shares[:, :, None], 0.0), axis=1)
+    all_shares = lax.all_gather(spread.T, ("ep", "tp"), axis=0).reshape(
+        n_ep, n_tp, n_ep, rows_exp
+    )
+    expert_shares = lax.dynamic_index_in_dim(all_shares, my_ep, axis=2, keepdims=False)
+
+    rows_mix = conv_x.shape[0]
+    reach_rows = conv_taps.shape[0] - 1
+    mixed_u = (conv_c.astype(jnp.float32) * conv_x.astype(jnp.float32)).astype(jnp.bfloat16)
+    before = shifted(mixed_u[rows_mix - reach_rows :], ("ep", "tp"), 1)
+    extended = jnp.concatenate([before, mixed_u], axis=0)
+    filtered = jnp.zeros(mixed_u.shape, jnp.float32)
+    for shift_tap in range(reach_rows + 1):
+        filtered = filtered + conv_taps[shift_tap][None, :] * extended[
+            shift_tap : shift_tap + rows_mix
+        ].astype(jnp.float32)
+    gated_rows = (conv_b.astype(jnp.float32) * filtered).astype(jnp.bfloat16)
+    mixed_out = None
+    for first, piece in pieces:
+        part = jnp.dot(
+            lax.dynamic_slice_in_dim(gated_rows, first, piece.shape[0], axis=1),
+            piece,
+            preferred_element_type=jnp.float32,
+        )
+        mixed_out = part if mixed_out is None else mixed_out + part
+    mixed_a = mixed_out.astype(jnp.bfloat16)
+
+    weight_gate = w_gate[0]
+    weight_up = w_up[0]
+    weight_down = w_down[0]
+    held = normed
+    total = None
+    for back in range(n_ep):
+        if back:
+            held = turned(held, "ep", 1)
+        far = swapped(held, "tp", 2)
+        rows = jnp.concatenate([held, far, swapped(held, "tp", 1), swapped(far, "tp", 1)], axis=0)
+        chunk_shares = lax.dynamic_index_in_dim(
+            expert_shares, (my_ep - back) % n_ep, axis=0, keepdims=False
+        )
+        factor = jnp.concatenate(
+            [
+                lax.dynamic_index_in_dim(chunk_shares, my_tp ^ mask, axis=0, keepdims=False)
+                for mask in (0, 2, 1, 3)
+            ]
+        )
+        hidden = expert_hidden(rows, weight_gate, weight_up)
+        partial = (
+            jnp.dot(hidden, weight_down, preferred_element_type=jnp.float32) * factor[:, None]
+        ).astype(jnp.bfloat16)
+        lane = 2 * rows_exp
+        from_near = swapped(partial[lane:], "tp", 1)
+        pair = (
+            partial[:lane].astype(jnp.float32) + from_near.astype(jnp.float32)
+        ).astype(jnp.bfloat16)
+        from_far = swapped(pair[rows_exp:], "tp", 2)
+        summed = (
+            pair[:rows_exp].astype(jnp.float32) + from_far.astype(jnp.float32)
+        ).astype(jnp.bfloat16)
+        if back:
+            summed = turned(summed, "ep", -back)
+        total = (
+            summed.astype(jnp.float32) if total is None else total + summed.astype(jnp.float32)
+        )
+    return (mixed_a, total.astype(jnp.bfloat16))
+
+
+def planned(mesh):
+    def body(*args):
+        experts = mesh.shape["ep"]
+        rows_exp = args[7].shape[0]
+        capacity = 2 * rows_exp * TOPK // experts
+        dense = capacity >= rows_exp and mesh.shape["tp"] == 4 and mesh.shape["grp"] == 2
+        return (dense_per_device if dense else per_device)(*args)
+
+    return body
+
+
 def solution(mesh):
     return jax.shard_map(
-        per_device,
+        planned(mesh),
         mesh=mesh,
         in_specs=(
             P(("grp", "ep", "tp"), None),

time: 307 us -> 216 us (0.70)
  waiting for transfers between devices: 179 us -> 79.7 us
  blocking collectives: 54.6 us -> 21.5 us
  matrix products: 28.9 us -> 46.1 us
  local copies, waits for them, and re-layouts: 12.9 us -> 30.1 us
  starting transfers between devices: 6.22 us -> 21.6 us
  between operations: 13.9 us -> 1.23 us
  other arithmetic: 10.5 us -> 14.9 us
    all_gather x2 -> x0, waiting for transfers between devices: 108 us -> none  [the longest x1 57.6 us: per_device(): lax.all_gather(arrived, 'tp', axis=0, tiled=True)]
    ppermute x0 -> x31, waiting for transfers between devices: none -> 79.7 us  [the longest x25 48.4 us: swapped(): lax.ppermute(x, axis, [(i, i ^ mask) for i in range(lax.axis_size(axis))])]
    reduce_scatter x1 -> x0, waiting for transfers between devices: 70.8 us -> none  [per_device(): lax.psum_scatter(jnp.dot(hidden, weight_down, preferred_element_type=jnp....]
    all_to_all x1 -> x0, blocking collectives: 54.6 us -> none  [per_device(): lax.all_to_all(outgoing, 'ep', split_axis=0, concat_axis=0, tiled=True)]
    all_gather x0 -> x1, blocking collectives: none -> 21.5 us  [dense_per_device(): lax.all_gather(spread.T, ('ep', 'tp'), axis=0)]
    dot_general x2 -> x13, matrix products: 21.8 us -> 43.2 us  [the longest x4 22.6 us: dense_per_device(): jnp.dot(hidden, weight_down, preferred_element_type=jnp.float32)]
    ppermute x0 -> x31, starting transfers between devices: none -> 19.2 us  [the longest x25 14.6 us: swapped(): lax.ppermute(x, axis, [(i, i ^ mask) for i in range(lax.axis_size(axis))])]
    unnamed x13 -> x59, local copies, waits for them, and re-layouts: 1.88 us -> 16.8 us
  transfers between devices with their start and end apart: 5 -> 32, of which waited for: 4 -> 7; matrix products, arithmetic and copies ran while one was open for 4% -> 37% of each run, Pallas kernels for 0% -> 0%
where the time goes in v1:
time: 216 us; the launch traced here: 215 us
  waiting for transfers between devices  79.7 us (37%)
  matrix products  46.1 us (21%)
  local copies, waits for them, and re-layouts  30.1 us (14%)
  starting transfers between devices  21.6 us (10%)
  blocking collectives  21.5 us (10%)
  other arithmetic  14.9 us (7%)
    ppermute x25, waiting for transfers between devices, swapped(): lax.ppermute(x, axis, [(i, i ^ mask) for i in range(lax.axis_size(axis))])  48.4 us
    ppermute x6, waiting for transfers between devices, turned(): return lax.ppermute(x, axis, [(i, (i + by) % size) for i in range(size)])  31.3 us
    dot_general x4, matrix products, dense_per_device(): jnp.dot(hidden, weight_down, preferred_element_type=jnp.float32)  22.6 us
    all_gather x1, blocking collectives, dense_per_device(): lax.all_gather(spread.T, ('ep', 'tp'), axis=0)  21.5 us
    unnamed x59, local copies, waits for them, and re-layouts  16.8 us
    dot_general x6, matrix products, dense_per_device(): jnp.dot(lax.dynamic_slice_in_dim(gated_rows, first, piece.shape[0], axis=...  16.1 us
    ppermute x25, starting transfers between devices, swapped(): lax.ppermute(x, axis, [(i, i ^ mask) for i in range(lax.axis_size(axis))])  14.6 us
    slice x4, local copies, waits for them, and re-layouts, dense_per_device(): from_near = swapped(partial[lane:], 'tp', 1)  8.81 us
  transfers between devices with their start and end apart: 32, of which 7 were waited for; matrix products, arithmetic and copies ran while one was open for 37% of the time, Pallas kernels for 0%

profile of v1, /device:TPU:0, one launch (start us, length us, event | category | flops | bytes accessed | tf_op | source)
XLA Modules:
  0.0 215.1 jit_solution(15289529375245436200)
XLA Ops:
  2.1 2.0 fusion.6
  4.1 3.1 %collective-permute-start.11 = (bf16[128,2048]{1,0:T(8,128)(2,1)}, bf16[128,2048]{1,0:T(8,128)(2,1)}, u32[]{:S(2)}, u32[]{:S(2)}) collective-permute-start(bf16[128,2048]{1,0:T(8,128)(2,1)} %fusion.6), channel_id=1, source_target_pairs={{0,4},{4,8},{8,12},{12,0},{1,5},{5,9},{9,13},{13,1},{2,6},{6,10},{... | collective-permute-start | bytes 1572872 | tf_op jit(solution)/shard_map/ppermute | solution.py:107
  10.3 2.4 %collective-permute-start = (bf16[2,2048]{1,0:T(2,128)(2,1)S(1)}, bf16[2,2048]{1,0:T(2,128)(2,1)S(1)}, u32[]{:S(2)}, u32[]{:S(2)}) collective-permute-start(bf16[2,2048]{1,0:T(2,128)(2,1)S(1)} %slice.88), channel_id=1, source_target_pairs={{0,1},{1,2},{2,3},{3,4},{4,5},{5,6},{6,7},{7,8},{8,9},{9,10},{10,1... | collective-permute-start | bytes 24584 | tf_op jit(solution)/shard_map/ppermute | solution.py:13
  13.0 21.5 %all-gather.1 = f32[16,4,128]{2,1,0:T(4,128)S(1)} all-gather(f32[1,4,128]{2,1,0:T(4,128)S(1)} %bitcast.98), channel_id=2, replica_groups=mesh['grp'=2,'ep'=4,'tp'=4] {'ep','tp'}, dimensions={0}, use_global_device_ids=true | all-gather | bytes 34816 | tf_op jit(solution)/shard_map/all_gather | solution.py:160
  34.5 2.3 %constant_dynamic-slice_fusion.16 = bf16[256,2048]{1,0:T(8,128)(2,1)} fusion(bf16[512,2048]{1,0:T(8,128)(2,1)} %param.16, s32[]{:T(128)S(6)} %select_n.107), kind=kLoop, calls=%fused_computation.99 | loop fusion | bytes 2097156 | tf_op jit(solution)/shard_map/dynamic_slice | solution.py:115
  38.4 2.6 %fusion.48 = f32[256,2048]{1,0:T(8,128)S(1)} fusion(bf16[512,2048]{1,0:T(8,128)(2,1)} %param.16, bf16[256,2048]{1,0:T(8,128)(2,1)S(1)} %multiply_convert_fusion.4, s32[]{:T(128)S(6)} %select_n.104), kind=kOutput, calls=%fused_computation.60 | convolution fusion | flops 536870912 | bytes 4456452 | tf_op jit(solution)/shard_map/dot_general | solution.py:178
  41.1 2.0 collective-permute-start.12
  43.0 1.9 constant_dynamic-update-slice_fusion.3
  45.8 2.9 %fusion.25 = f32[512,256]{1,0:T(8,128)} fusion(bf16[1,2048,256]{2,1,0:T(8,128)(2,1)S(1)} %copy-done.23, bf16[128,2048]{1,0:T(8,128)(2,1)S(1)} %collective-permute-done.8, bf16[128,2048]{1,0:T(8,128)(2,1)} %collective-permute-done.7, bf16[128,2048]{1,0:T(8,128)(2,1)} %collective-permute-done.6, bf16[128,2048]{1,0:T(8,128)(2,1)} %fusion.6), kind=kOutput, calls=%fused_computation.44 | convolution fusion | flops 545259520 | bytes 3670016 | tf_op jit(solution)/shard_map/dot_general | solution.py:30
  48.7 5.6 %multiply_convert_fusion.3 = bf16[512,2048]{1,0:T(8,128)(2,1)} fusion(f32[512]{0:T(512)S(1)} %pad_maximum_fusion.8, bf16[1,256,2048]{2,1,0:T(8,128)(2,1)S(1)} %copy-done, f32[512,256]{1,0:T(8,128)} %fusion.25, bf16[1,2048,256]{2,1,0:T(8,128)(2,1)} %param.22, bf16[128,2048]{1,0:T(8,128)(2,1)} %copy-done.24, bf16[128,2048]{1,0:T(8,128)(2,1)} %collective-permute-done.7, ...), kind=kOutput, calls=%fused_computation.3 | convolution fusion | flops 1085014016 | bytes 6817792 | tf_op jit(solution)/shard_map/dot_general | solution.py:207
  54.3 2.5 %slice.92 = bf16[256,2048]{1,0:T(8,128)(2,1)} slice(bf16[512,2048]{1,0:T(8,128)(2,1)} %multiply_convert_fusion.3), slice={[256:512], [0:2048]} | slice | bytes 2097152 | tf_op jit(solution)/shard_map/slice | solution.py:210
  56.8 17.3 %collective-permute-done.12 = bf16[128,2048]{1,0:T(8,128)(2,1)} collective-permute-done((bf16[128,2048]{1,0:T(8,128)(2,1)}, bf16[128,2048]{1,0:T(8,128)(2,1)}, u32[]{:S(2)}, u32[]{:S(2)}) %collective-permute-start.12) | collective-permute-done | bytes 524320 | tf_op jit(solution)/shard_map/ppermute | solution.py:102
  75.7 1.9 constant_dynamic-update-slice_fusion.7
  79.1 3.1 %fusion.54 = f32[256,2048]{1,0:T(8,128)} fusion(bf16[256,2048]{1,0:T(8,128)(2,1)} %collective-permute-done.2, bf16[256,2048]{1,0:T(8,128)(2,1)} %copy-done.3, s32[]{:T(128)S(6)} %select_n.106), kind=kOutput, calls=%fused_computation.66 | convolution fusion | flops 268435456 | bytes 3276804 | tf_op jit(solution)/shard_map/dot_general | solution.py:178
  85.1 5.6 %multiply_convert_fusion.2 = bf16[512,2048]{1,0:T(8,128)(2,1)} fusion(f32[512]{0:T(512)S(1)} %pad_maximum_fusion.9, bf16[1,256,2048]{2,1,0:T(8,128)(2,1)S(1)} %copy-done, f32[512,256]{1,0:T(8,128)} %fusion.15, bf16[512,2048]{1,0:T(8,128)(2,1)} %copy-done.16, bf16[1,2048,256]{2,1,0:T(8,128)(2,1)} %param.21), kind=kOutput, calls=%fused_computation.2 | convolution fusion | flops 1076625408 | bytes 6817792 | tf_op jit(solution)/shard_map/dot_general | solution.py:207
  91.8 1.9 constant_dynamic-update-slice_fusion.6
  93.7 2.5 %slice.96 = bf16[256,2048]{1,0:T(8,128)(2,1)} slice(bf16[512,2048]{1,0:T(8,128)(2,1)} %multiply_convert_fusion.2), slice={[256:512], [0:2048]} | slice | bytes 2097152 | tf_op jit(solution)/shard_map/slice | solution.py:210
  96.1 2.5 %collective-permute-done.25 = bf16[128,2048]{1,0:T(8,128)(2,1)} collective-permute-done((bf16[128,2048]{1,0:T(8,128)(2,1)}, bf16[128,2048]{1,0:T(8,128)(2,1)}, u32[]{:S(2)}, u32[]{:S(2)}) %collective-permute-start.25) | collective-permute-done | bytes 524320 | tf_op jit(solution)/shard_map/ppermute | solution.py:107
  100.1 1.9 constant_dynamic-update-slice_fusion.11
  108.3 2.6 %add_convert_fusion.3 = bf16[256,2048]{1,0:T(8,128)(2,1)} fusion(bf16[256,2048]{1,0:T(8,128)(2,1)} %collective-permute-done.9, bf16[512,2048]{1,0:T(8,128)(2,1)S(1)} %copy-done.6), kind=kLoop, calls=%fused_computation.14 | loop fusion | flops 2097152 | bytes 3145728 | tf_op jit(solution)/shard_map/convert_element_type | solution.py:213
  110.9 5.7 %multiply_convert_fusion.1 = bf16[512,2048]{1,0:T(8,128)(2,1)} fusion(f32[512]{0:T(512)S(1)} %pad_maximum_fusion.10, bf16[1,256,2048]{2,1,0:T(8,128)(2,1)S(1)} %copy-done, f32[512,256]{1,0:T(8,128)} %fusion.13, bf16[512,2048]{1,0:T(8,128)(2,1)} %copy-done.14, bf16[1,2048,256]{2,1,0:T(8,128)(2,1)} %param.21), kind=kOutput, calls=%fused_computation.1 | convolution fusion | flops 1076625408 | bytes 6817792 | tf_op jit(solution)/shard_map/dot_general | solution.py:207
  116.6 2.5 %slice.100 = bf16[256,2048]{1,0:T(8,128)(2,1)} slice(bf16[512,2048]{1,0:T(8,128)(2,1)} %multiply_convert_fusion.1), slice={[256:512], [0:2048]} | slice | bytes 2097152 | tf_op jit(solution)/shard_map/slice | solution.py:210
  119.1 1.9 slice.94
  121.0 4.0 %fusion = f32[256,2048]{1,0:T(8,128)} fusion(f32[256,2048]{1,0:T(8,128)S(1)} %copy-done.1, f32[256,2048]{1,0:T(8,128)S(1)} %fusion.48, bf16[512,2048]{1,0:T(8,128)(2,1)} %collective-permute-done.1, bf16[256,2048]{1,0:T(8,128)(2,1)} %copy-done.3, s32[]{:T(128)S(6)} %select_n.105), kind=kOutput, calls=%fused_computation.5 | convolution fusion | flops 537919488 | bytes 8650756 | tf_op jit(solution)/shard_map/dot_general | solution.py:178
  131.8 5.6 %multiply_convert_fusion = bf16[512,2048]{1,0:T(8,128)(2,1)} fusion(f32[512]{0:T(512)S(1)} %pad_maximum_fusion.11, bf16[1,256,2048]{2,1,0:T(8,128)(2,1)S(1)} %copy-done, f32[512,256]{1,0:T(8,128)} %fusion.11, bf16[512,2048]{1,0:T(8,128)(2,1)} %copy-done.12, bf16[1,2048,256]{2,1,0:T(8,128)(2,1)} %param.21), kind=kOutput, calls=%fused_computation | convolution fusion | flops 1076625408 | bytes 6817792 | tf_op jit(solution)/shard_map/dot_general | solution.py:207
  145.7 10.4 %collective-permute-done.16 = bf16[128,2048]{1,0:T(8,128)(2,1)S(1)} collective-permute-done((bf16[128,2048]{1,0:T(8,128)(2,1)S(1)}, bf16[128,2048]{1,0:T(8,128)(2,1)S(1)}, u32[]{:S(2)}, u32[]{:S(2)}) %collective-permute-start.16) | collective-permute-done | bytes 524320 | tf_op jit(solution)/shard_map/ppermute | solution.py:102
  158.0 9.4 %collective-permute-done.23 = bf16[128,2048]{1,0:T(8,128)(2,1)S(1)} collective-permute-done((bf16[128,2048]{1,0:T(8,128)(2,1)S(1)}, bf16[128,2048]{1,0:T(8,128)(2,1)S(1)}, u32[]{:S(2)}, u32[]{:S(2)}) %collective-permute-start.23) | collective-permute-done | bytes 524320 | tf_op jit(solution)/shard_map/ppermute | solution.py:102
  167.9 10.2 %collective-permute-done.30 = bf16[128,2048]{1,0:T(8,128)(2,1)S(1)} collective-permute-done((bf16[128,2048]{1,0:T(8,128)(2,1)S(1)}, bf16[128,2048]{1,0:T(8,128)(2,1)S(1)}, u32[]{:S(2)}, u32[]{:S(2)}) %collective-permute-start.30) | collective-permute-done | bytes 524320 | tf_op jit(solution)/shard_map/ppermute | solution.py:102
  179.3 1.8 fusion.1
  181.2 2.8 %fusion.2 = bf16[256,2048]{1,0:T(8,128)(2,1)} fusion(f32[256,2048]{1,0:T(8,128)S(1)} %fusion.1, bf16[256,2048]{1,0:T(8,128)(2,1)} %collective-permute-done.5, bf16[256,2048]{1,0:T(8,128)(2,1)} %copy-done.3, s32[]{:T(128)S(6)} %select_n.110), kind=kOutput, calls=%fused_computation.9 | convolution fusion | flops 269484032 | bytes 4325380 | tf_op jit(solution)/shard_map/dot_general | solution.py:178
  184.0 28.8 %collective-permute-done.24 = bf16[128,2048]{1,0:T(8,128)(2,1)S(1)} collective-permute-done((bf16[128,2048]{1,0:T(8,128)(2,1)S(1)}, bf16[128,2048]{1,0:T(8,128)(2,1)S(1)}, u32[]{:S(2)}, u32[]{:S(2)}) %collective-permute-start.24) | collective-permute-done | bytes 524320 | tf_op jit(solution)/shard_map/ppermute | solution.py:107
  212.8 2.3 %add_convert_fusion.4 = bf16[128,2048]{1,0:T(8,128)(2,1)} fusion(bf16[128,2048]{1,0:T(8,128)(2,1)S(1)} %collective-permute-done.31, bf16[128,2048]{1,0:T(8,128)(2,1)S(1)} %collective-permute-done.24, bf16[128,2048]{1,0:T(8,128)(2,1)S(1)} %collective-permute-done.17, bf16[128,2048]{1,0:T(8,128)(2,1)} %collective-permute-done.10, ...), kind=kLoop, calls=%fused_computation.46 | loop fusion | flops 3145728 | bytes 3145728 | tf_op jit(solution)/shard_map/convert_element_type | solution.py:223
  (141 shorter events, 40.5 us)
Async XLA Ops:
  4.1 36.9 %collective-permute-start.11 = (bf16[128,2048]{1,0:T(8,128)(2,1)}, bf16[128,2048]{1,0:T(8,128)(2,1)}, u32[]{:S(2)}, u32[]{:S(2)}) collective-permute-start(bf16[128,2048]{1,0:T(8,128)(2,1)} %fusion.6), channel_id=1, source_target_pairs={{0,4},{4,8},{8,12},{12,0},{1,5},{5,9},{9,13},{13,1},{2,6},{6,10},{... | collective-permute-start | bytes 1572872 | tf_op jit(solution)/shard_map/ppermute | solution.py:107
  7.2 30.9 %collective-permute-start.6 = (bf16[128,2048]{1,0:T(8,128)(2,1)}, bf16[128,2048]{1,0:T(8,128)(2,1)}, u32[]{:S(2)}, u32[]{:S(2)}) collective-permute-start(bf16[128,2048]{1,0:T(8,128)(2,1)} %fusion.6), channel_id=1, source_target_pairs={{0,2},{1,3},{2,0},{3,1},{4,6},{5,7},{6,4},{7,5},{8,10},{9,11},{10,... | collective-permute-start | bytes 1572872 | tf_op jit(solution)/shard_map/ppermute | solution.py:102
  8.6 36.3 %collective-permute-start.7 = (bf16[128,2048]{1,0:T(8,128)(2,1)}, bf16[128,2048]{1,0:T(8,128)(2,1)}, u32[]{:S(2)}, u32[]{:S(2)}) collective-permute-start(bf16[128,2048]{1,0:T(8,128)(2,1)} %fusion.6), channel_id=1, source_target_pairs={{0,1},{1,0},{2,3},{3,2},{4,5},{5,4},{6,7},{7,6},{8,9},{9,8},{10,11... | collective-permute-start | bytes 1572872 | tf_op jit(solution)/shard_map/ppermute | solution.py:102
  10.3 26.7 %collective-permute-start = (bf16[2,2048]{1,0:T(2,128)(2,1)S(1)}, bf16[2,2048]{1,0:T(2,128)(2,1)S(1)}, u32[]{:S(2)}, u32[]{:S(2)}) collective-permute-start(bf16[2,2048]{1,0:T(2,128)(2,1)S(1)} %slice.88), channel_id=1, source_target_pairs={{0,1},{1,2},{2,3},{3,4},{4,5},{5,6},{6,7},{7,8},{8,9},{9,10},{10,1... | collective-permute-start | bytes 24584 | tf_op jit(solution)/shard_map/ppermute | solution.py:13
  12.7 108.2 %collective-permute-start.1 = (bf16[512,2048]{1,0:T(8,128)(2,1)}, bf16[512,2048]{1,0:T(8,128)(2,1)}, u32[]{:S(2)}, u32[]{:S(2)}) collective-permute-start(bf16[512,2048]{1,0:T(8,128)(2,1)} %param.16), channel_id=1, source_target_pairs={{0,1},{1,0},{2,3},{3,2},{4,5},{5,4},{6,7},{7,6},{8,9},{9,8},{10,11... | collective-permute-start | bytes 6291464 | tf_op jit(solution)/shard_map/ppermute | solution.py:102
  37.0 42.0 %collective-permute-start.2 = (bf16[256,2048]{1,0:T(8,128)(2,1)}, bf16[256,2048]{1,0:T(8,128)(2,1)}, u32[]{:S(2)}, u32[]{:S(2)}) collective-permute-start(bf16[256,2048]{1,0:T(8,128)(2,1)} %constant_dynamic-slice_fusion.16), channel_id=1, source_target_pairs={{0,2},{1,3},{2,0},{3,1},{4,6},{5,7},{6,4},{7,5},{8,10},{9,11},{10,... | collective-permute-start | bytes 3145736 | tf_op jit(solution)/shard_map/ppermute | solution.py:102
  38.0 6.9 %collective-permute-start.8 = (bf16[128,2048]{1,0:T(8,128)(2,1)}, bf16[128,2048]{1,0:T(8,128)(2,1)S(1)}, u32[]{:S(2)}, u32[]{:S(2)}) collective-permute-start(bf16[128,2048]{1,0:T(8,128)(2,1)} %collective-permute-done.6), channel_id=1, source_target_pairs={{0,1},{1,0},{2,3},{3,2},{4,5},{5,4},{6,7},{7,6},{8,9},{9,8},{10,11... | collective-permute-start | bytes 1572872 | tf_op jit(solution)/shard_map/ppermute | solution.py:102
  41.1 33.0 %collective-permute-start.12 = (bf16[128,2048]{1,0:T(8,128)(2,1)}, bf16[128,2048]{1,0:T(8,128)(2,1)}, u32[]{:S(2)}, u32[]{:S(2)}) collective-permute-start(bf16[128,2048]{1,0:T(8,128)(2,1)} %collective-permute-done.11), channel_id=1, source_target_pairs={{0,2},{1,3},{2,0},{3,1},{4,6},{5,7},{6,4},{7,5},{8,10},{9,11},{10,... | collective-permute-start | bytes 1572872 | tf_op jit(solution)/shard_map/ppermute | solution.py:102
  45.0 32.7 %collective-permute-start.13 = (bf16[128,2048]{1,0:T(8,128)(2,1)}, bf16[128,2048]{1,0:T(8,128)(2,1)}, u32[]{:S(2)}, u32[]{:S(2)}) collective-permute-start(bf16[128,2048]{1,0:T(8,128)(2,1)} %collective-permute-done.11), channel_id=1, source_target_pairs={{0,1},{1,0},{2,3},{3,2},{4,5},{5,4},{6,7},{7,6},{8,9},{9,8},{10,11... | collective-permute-start | bytes 1572872 | tf_op jit(solution)/shard_map/ppermute | solution.py:102
  45.0 30.2 %collective-permute-start.18 = (bf16[128,2048]{1,0:T(8,128)(2,1)}, bf16[128,2048]{1,0:T(8,128)(2,1)}, u32[]{:S(2)}, u32[]{:S(2)}) collective-permute-start(bf16[128,2048]{1,0:T(8,128)(2,1)} %collective-permute-done.11), channel_id=1, source_target_pairs={{0,4},{4,8},{8,12},{12,0},{1,5},{5,9},{9,13},{13,1},{2,6},{6,10},{... | collective-permute-start | bytes 1572872 | tf_op jit(solution)/shard_map/ppermute | solution.py:107
  74.1 32.5 %collective-permute-start.9 = (bf16[256,2048]{1,0:T(8,128)(2,1)}, bf16[256,2048]{1,0:T(8,128)(2,1)}, u32[]{:S(2)}, u32[]{:S(2)}) collective-permute-start(bf16[256,2048]{1,0:T(8,128)(2,1)} %slice.92), channel_id=1, source_target_pairs={{0,1},{1,0},{2,3},{3,2},{4,5},{5,4},{6,7},{7,6},{8,9},{9,8},{10,11... | collective-permute-start | bytes 3145736 | tf_op jit(solution)/shard_map/ppermute | solution.py:102
  75.2 7.0 %collective-permute-start.14 = (bf16[128,2048]{1,0:T(8,128)(2,1)}, bf16[128,2048]{1,0:T(8,128)(2,1)S(1)}, u32[]{:S(2)}, u32[]{:S(2)}) collective-permute-start(bf16[128,2048]{1,0:T(8,128)(2,1)} %collective-permute-done.12), channel_id=1, source_target_pairs={{0,1},{1,0},{2,3},{3,2},{4,5},{5,4},{6,7},{7,6},{8,9},{9,8},{10,11... | collective-permute-start | bytes 1572872 | tf_op jit(solution)/shard_map/ppermute | solution.py:102
  77.6 14.2 %collective-permute-start.19 = (bf16[128,2048]{1,0:T(8,128)(2,1)}, bf16[128,2048]{1,0:T(8,128)(2,1)}, u32[]{:S(2)}, u32[]{:S(2)}) collective-permute-start(bf16[128,2048]{1,0:T(8,128)(2,1)} %collective-permute-done.18), channel_id=1, source_target_pairs={{0,2},{1,3},{2,0},{3,1},{4,6},{5,7},{6,4},{7,5},{8,10},{9,11},{10,... | collective-permute-start | bytes 1572872 | tf_op jit(solution)/shard_map/ppermute | solution.py:102
  79.0 23.0 %collective-permute-start.20 = (bf16[128,2048]{1,0:T(8,128)(2,1)}, bf16[128,2048]{1,0:T(8,128)(2,1)}, u32[]{:S(2)}, u32[]{:S(2)}) collective-permute-start(bf16[128,2048]{1,0:T(8,128)(2,1)} %collective-permute-done.18), channel_id=1, source_target_pairs={{0,1},{1,0},{2,3},{3,2},{4,5},{5,4},{6,7},{7,6},{8,9},{9,8},{10,11... | collective-permute-start | bytes 1572872 | tf_op jit(solution)/shard_map/ppermute | solution.py:102
  82.2 16.4 %collective-permute-start.25 = (bf16[128,2048]{1,0:T(8,128)(2,1)}, bf16[128,2048]{1,0:T(8,128)(2,1)}, u32[]{:S(2)}, u32[]{:S(2)}) collective-permute-start(bf16[128,2048]{1,0:T(8,128)(2,1)} %collective-permute-done.18), channel_id=1, source_target_pairs={{0,4},{4,8},{8,12},{12,0},{1,5},{5,9},{9,13},{13,1},{2,6},{6,10},{... | collective-permute-start | bytes 1572872 | tf_op jit(solution)/shard_map/ppermute | solution.py:107
  91.8 11.3 %collective-permute-start.21 = (bf16[128,2048]{1,0:T(8,128)(2,1)}, bf16[128,2048]{1,0:T(8,128)(2,1)S(1)}, u32[]{:S(2)}, u32[]{:S(2)}) collective-permute-start(bf16[128,2048]{1,0:T(8,128)(2,1)} %collective-permute-done.19), channel_id=1, source_target_pairs={{0,1},{1,0},{2,3},{3,2},{4,5},{5,4},{6,7},{7,6},{8,9},{9,8},{10,11... | collective-permute-start | bytes 1572872 | tf_op jit(solution)/shard_map/ppermute | solution.py:102
  98.6 27.8 %collective-permute-start.4 = (bf16[256,2048]{1,0:T(8,128)(2,1)}, bf16[256,2048]{1,0:T(8,128)(2,1)}, u32[]{:S(2)}, u32[]{:S(2)}) collective-permute-start(bf16[256,2048]{1,0:T(8,128)(2,1)} %collective-permute-done.2), channel_id=1, source_target_pairs={{0,16},{16,0},{1,17},{17,1},{2,18},{18,2},{3,19},{19,3},{4,20},{20... | collective-permute-start | bytes 3145736 | tf_op jit(solution)/shard_map/ppermute | solution.py:102
  102.0 76.2 %collective-permute-start.3 = (bf16[256,2048]{1,0:T(8,128)(2,1)}, bf16[256,2048]{1,0:T(8,128)(2,1)}, u32[]{:S(2)}, u32[]{:S(2)}) collective-permute-start(bf16[256,2048]{1,0:T(8,128)(2,1)} %collective-permute-done.2), channel_id=1, source_target_pairs={{0,1},{1,0},{2,3},{3,2},{4,5},{5,4},{6,7},{7,6},{8,9},{9,8},{10,11... | collective-permute-start | bytes 3145736 | tf_op jit(solution)/shard_map/ppermute | solution.py:102
  103.1 35.8 %collective-permute-start.15 = (bf16[256,2048]{1,0:T(8,128)(2,1)}, bf16[256,2048]{1,0:T(8,128)(2,1)}, u32[]{:S(2)}, u32[]{:S(2)}) collective-permute-start(bf16[256,2048]{1,0:T(8,128)(2,1)} %slice.96), channel_id=1, source_target_pairs={{0,1},{1,0},{2,3},{3,2},{4,5},{5,4},{6,7},{7,6},{8,9},{9,8},{10,11... | collective-permute-start | bytes 3145736 | tf_op jit(solution)/shard_map/ppermute | solution.py:102
  106.6 18.3 %collective-permute-start.26 = (bf16[128,2048]{1,0:T(8,128)(2,1)}, bf16[128,2048]{1,0:T(8,128)(2,1)}, u32[]{:S(2)}, u32[]{:S(2)}) collective-permute-start(bf16[128,2048]{1,0:T(8,128)(2,1)} %collective-permute-done.25), channel_id=1, source_target_pairs={{0,2},{1,3},{2,0},{3,1},{4,6},{5,7},{6,4},{7,5},{8,10},{9,11},{10,... | collective-permute-start | bytes 1572872 | tf_op jit(solution)/shard_map/ppermute | solution.py:102
  121.0 7.5 %collective-permute-start.27 = (bf16[128,2048]{1,0:T(8,128)(2,1)}, bf16[128,2048]{1,0:T(8,128)(2,1)S(1)}, u32[]{:S(2)}, u32[]{:S(2)}) collective-permute-start(bf16[128,2048]{1,0:T(8,128)(2,1)} %collective-permute-done.25), channel_id=1, source_target_pairs={{0,1},{1,0},{2,3},{3,2},{4,5},{5,4},{6,7},{7,6},{8,9},{9,8},{10,11... | collective-permute-start | bytes 1572872 | tf_op jit(solution)/shard_map/ppermute | solution.py:102
  124.9 16.3 %collective-permute-start.22 = (bf16[256,2048]{1,0:T(8,128)(2,1)}, bf16[256,2048]{1,0:T(8,128)(2,1)}, u32[]{:S(2)}, u32[]{:S(2)}) collective-permute-start(bf16[256,2048]{1,0:T(8,128)(2,1)} %slice.100), channel_id=1, source_target_pairs={{0,1},{1,0},{2,3},{3,2},{4,5},{5,4},{6,7},{7,6},{8,9},{9,8},{10,11... | collective-permute-start | bytes 3145736 | tf_op jit(solution)/shard_map/ppermute | solution.py:102
  126.4 2.4 %collective-permute-start.28 = (bf16[128,2048]{1,0:T(8,128)(2,1)}, bf16[128,2048]{1,0:T(8,128)(2,1)S(1)}, u32[]{:S(2)}, u32[]{:S(2)}) collective-permute-start(bf16[128,2048]{1,0:T(8,128)(2,1)} %collective-permute-done.26), channel_id=1, source_target_pairs={{0,1},{1,0},{2,3},{3,2},{4,5},{5,4},{6,7},{7,6},{8,9},{9,8},{10,11... | collective-permute-start | bytes 1572872 | tf_op jit(solution)/shard_map/ppermute | solution.py:102
  128.5 55.5 %collective-permute-start.10 = (bf16[128,2048]{1,0:T(8,128)(2,1)}, bf16[128,2048]{1,0:T(8,128)(2,1)}, u32[]{:S(2)}, u32[]{:S(2)}) collective-permute-start(bf16[128,2048]{1,0:T(8,128)(2,1)} %slice.94), channel_id=1, source_target_pairs={{0,2},{1,3},{2,0},{3,1},{4,6},{5,7},{6,4},{7,5},{8,10},{9,11},{10,... | collective-permute-start | bytes 1572872 | tf_op jit(solution)/shard_map/ppermute | solution.py:102
  128.9 52.3 %collective-permute-start.5 = (bf16[256,2048]{1,0:T(8,128)(2,1)}, bf16[256,2048]{1,0:T(8,128)(2,1)}, u32[]{:S(2)}, u32[]{:S(2)}) collective-permute-start(bf16[256,2048]{1,0:T(8,128)(2,1)} %collective-permute-done.4), channel_id=1, source_target_pairs={{0,1},{1,0},{2,3},{3,2},{4,5},{5,4},{6,7},{7,6},{8,9},{9,8},{10,11... | collective-permute-start | bytes 3145736 | tf_op jit(solution)/shard_map/ppermute | solution.py:102
  138.9 5.8 %collective-permute-start.29 = (bf16[256,2048]{1,0:T(8,128)(2,1)S(1)}, bf16[256,2048]{1,0:T(8,128)(2,1)S(1)}, u32[]{:S(2)}, u32[]{:S(2)}) collective-permute-start(bf16[256,2048]{1,0:T(8,128)(2,1)S(1)} %slice.104), channel_id=1, source_target_pairs={{0,1},{1,0},{2,3},{3,2},{4,5},{5,4},{6,7},{7,6},{8,9},{9,8},{10,11... | collective-permute-start | bytes 3145736 | tf_op jit(solution)/shard_map/ppermute | solution.py:102
  141.2 14.9 %collective-permute-start.16 = (bf16[128,2048]{1,0:T(8,128)(2,1)S(1)}, bf16[128,2048]{1,0:T(8,128)(2,1)S(1)}, u32[]{:S(2)}, u32[]{:S(2)}) collective-permute-start(bf16[128,2048]{1,0:T(8,128)(2,1)S(1)} %slice.98), channel_id=1, source_target_pairs={{0,2},{1,3},{2,0},{3,1},{4,6},{5,7},{6,4},{7,5},{8,10},{9,11},{10,... | collective-permute-start | bytes 1572872 | tf_op jit(solution)/shard_map/ppermute | solution.py:102
  144.7 22.6 %collective-permute-start.23 = (bf16[128,2048]{1,0:T(8,128)(2,1)S(1)}, bf16[128,2048]{1,0:T(8,128)(2,1)S(1)}, u32[]{:S(2)}, u32[]{:S(2)}) collective-permute-start(bf16[128,2048]{1,0:T(8,128)(2,1)S(1)} %slice.102), channel_id=1, source_target_pairs={{0,2},{1,3},{2,0},{3,1},{4,6},{5,7},{6,4},{7,5},{8,10},{9,11},{10,... | collective-permute-start | bytes 1572872 | tf_op jit(solution)/shard_map/ppermute | solution.py:102
  156.1 22.0 %collective-permute-start.30 = (bf16[128,2048]{1,0:T(8,128)(2,1)S(1)}, bf16[128,2048]{1,0:T(8,128)(2,1)S(1)}, u32[]{:S(2)}, u32[]{:S(2)}) collective-permute-start(bf16[128,2048]{1,0:T(8,128)(2,1)S(1)} %slice.106), channel_id=1, source_target_pairs={{0,2},{1,3},{2,0},{3,1},{4,6},{5,7},{6,4},{7,5},{8,10},{9,11},{10,... | collective-permute-start | bytes 1572872 | tf_op jit(solution)/shard_map/ppermute | solution.py:102
  167.3 16.6 %collective-permute-start.17 = (bf16[128,2048]{1,0:T(8,128)(2,1)S(1)}, bf16[128,2048]{1,0:T(8,128)(2,1)S(1)}, u32[]{:S(2)}, u32[]{:S(2)}) collective-permute-start(bf16[128,2048]{1,0:T(8,128)(2,1)S(1)} %add_convert_fusion.7), channel_id=1, source_target_pairs={{0,12},{4,0},{8,4},{12,8},{1,13},{5,1},{9,5},{13,9},{2,14},{6,2},{... | collective-permute-start | bytes 1572872 | tf_op jit(solution)/shard_map/ppermute | solution.py:107
  178.1 34.7 %collective-permute-start.24 = (bf16[128,2048]{1,0:T(8,128)(2,1)S(1)}, bf16[128,2048]{1,0:T(8,128)(2,1)S(1)}, u32[]{:S(2)}, u32[]{:S(2)}) collective-permute-start(bf16[128,2048]{1,0:T(8,128)(2,1)S(1)} %add_convert_fusion.6), channel_id=1, source_target_pairs={{0,8},{4,12},{8,0},{12,4},{1,9},{5,13},{9,1},{13,5},{2,10},{6,14},... | collective-permute-start | bytes 1572872 | tf_op jit(solution)/shard_map/ppermute | solution.py:107
  178.2 34.6 %collective-permute-start.31 = (bf16[128,2048]{1,0:T(8,128)(2,1)S(1)}, bf16[128,2048]{1,0:T(8,128)(2,1)S(1)}, u32[]{:S(2)}, u32[]{:S(2)}) collective-permute-start(bf16[128,2048]{1,0:T(8,128)(2,1)S(1)} %add_convert_fusion.5), channel_id=1, source_target_pairs={{0,4},{4,8},{8,12},{12,0},{1,5},{5,9},{9,13},{13,1},{2,6},{6,10},{... | collective-permute-start | bytes 1572872 | tf_op jit(solution)/shard_map/ppermute | solution.py:107
  (25 other events, 292.3 us)

commit v2 on v1

--- a/solution.py
+++ b/solution.py
@@ -143,9 +143,7 @@
     w_down,
 ):
     n_ep = lax.axis_size("ep")
-    n_tp = lax.axis_size("tp")
     my_ep = lax.axis_index("ep")
-    my_tp = lax.axis_index("tp")
     rows_exp = route_b.shape[0]
     pieces = gathered_pieces(w_out)
     tokens_f = tokens_b.astype(jnp.float32)
@@ -155,12 +153,6 @@
         * norm_gain
     ).astype(jnp.bfloat16)
     shares = route_weights / jnp.sum(route_weights, axis=-1, keepdims=True)
-    named = route_b[:, :, None] == jnp.arange(n_ep, dtype=jnp.int32)[None, None, :]
-    spread = jnp.sum(jnp.where(named, shares[:, :, None], 0.0), axis=1)
-    all_shares = lax.all_gather(spread.T, ("ep", "tp"), axis=0).reshape(
-        n_ep, n_tp, n_ep, rows_exp
-    )
-    expert_shares = lax.dynamic_index_in_dim(all_shares, my_ep, axis=2, keepdims=False)
 
     rows_mix = conv_x.shape[0]
     reach_rows = conv_taps.shape[0] - 1
@@ -186,40 +178,50 @@
     weight_gate = w_gate[0]
     weight_up = w_up[0]
     weight_down = w_down[0]
-    held = normed
-    total = None
-    for back in range(n_ep):
-        if back:
-            held = turned(held, "ep", 1)
-        far = swapped(held, "tp", 2)
-        rows = jnp.concatenate([held, far, swapped(held, "tp", 1), swapped(far, "tp", 1)], axis=0)
-        chunk_shares = lax.dynamic_index_in_dim(
-            expert_shares, (my_ep - back) % n_ep, axis=0, keepdims=False
+
+    def expert(rows):
+        return jnp.dot(
+            expert_hidden(rows, weight_gate, weight_up),
+            weight_down,
+            preferred_element_type=jnp.float32,
         )
-        factor = jnp.concatenate(
-            [
-                lax.dynamic_index_in_dim(chunk_shares, my_tp ^ mask, axis=0, keepdims=False)
-                for mask in (0, 2, 1, 3)
-            ]
-        )
-        hidden = expert_hidden(rows, weight_gate, weight_up)
-        partial = (
-            jnp.dot(hidden, weight_down, preferred_element_type=jnp.float32) * factor[:, None]
-        ).astype(jnp.bfloat16)
-        lane = 2 * rows_exp
-        from_near = swapped(partial[lane:], "tp", 1)
-        pair = (
-            partial[:lane].astype(jnp.float32) + from_near.astype(jnp.float32)
-        ).astype(jnp.bfloat16)
-        from_far = swapped(pair[rows_exp:], "tp", 2)
-        summed = (
-            pair[:rows_exp].astype(jnp.float32) + from_far.astype(jnp.float32)
-        ).astype(jnp.bfloat16)
-        if back:
-            summed = turned(summed, "ep", -back)
-        total = (
-            summed.astype(jnp.float32) if total is None else total + summed.astype(jnp.float32)
-        )
+
+    helds = [normed]
+    for back in range(1, n_ep):
+        helds.append(turned(helds[-1], "ep", 1))
+    order = [*range(1, n_ep), 0]
+    if n_ep > 2:
+        helds[0], helds[2] = lax.optimization_barrier((helds[0], helds[2]))
+    pairs, sums, backs = [], [], []
+    for at, back in enumerate(order):
+        held = helds[back]
+        lane = jnp.concatenate([held, swapped(held, "tp", 2)], axis=0)
+        near = swapped(lane, "tp", 1)
+        if at >= 1:
+            near, pairs[at - 1] = lax.optimization_barrier((near, pairs[at - 1]))
+            from_far = swapped(pairs[at - 1][rows_exp:], "tp", 2)
+            sums.append(
+                (
+                    pairs[at - 1][:rows_exp].astype(jnp.float32) + from_far.astype(jnp.float32)
+                ).astype(jnp.bfloat16)
+            )
+        if at >= 2:
+            near, sums[at - 2] = lax.optimization_barrier((near, sums[at - 2]))
+            backs.append(turned(sums[at - 2], "ep", -order[at - 2]))
+        from_near = swapped(expert(near).astype(jnp.bfloat16), "tp", 1)
+        pairs.append((expert(lane) + from_near.astype(jnp.float32)).astype(jnp.bfloat16))
+    last, *backs = lax.optimization_barrier((pairs[-1], *backs))
+    from_far = swapped(last[rows_exp:], "tp", 2)
+    sums.append(
+        (last[:rows_exp].astype(jnp.float32) + from_far.astype(jnp.float32)).astype(jnp.bfloat16)
+    )
+    for at in range(len(backs), n_ep):
+        backs.append(turned(sums[at], "ep", -order[at]) if order[at] else sums[at])
+    total = jnp.zeros((rows_exp, D), jnp.float32)
+    for back, summed in zip(order, backs):
+        chosen = route_b == (my_ep + back) % n_ep
+        share = jnp.sum(jnp.where(chosen, shares, 0.0), axis=1, keepdims=True)
+        total = total + summed.astype(jnp.float32) * share
     return (mixed_a, total.astype(jnp.bfloat16))
 
 

time: 216 us -> 215 us (level)
  blocking collectives: 21.5 us -> 0 us
  matrix products: 46.1 us -> 60.5 us
  waiting for transfers between devices: 79.7 us -> 92.8 us
  local copies, waits for them, and re-layouts: 30.1 us -> 20.2 us
  starting transfers between devices: 21.6 us -> 26.6 us
    all_gather x1 -> x0, blocking collectives: 21.5 us -> none  [dense_per_device(): lax.all_gather(spread.T, ('ep', 'tp'), axis=0)]
    ppermute x6, waiting for transfers between devices: 31.3 us -> 43 us  [turned(): return lax.ppermute(x, axis, [(i, (i + by) % size) for i in range(size)])]
    unnamed x59 -> x40, local copies, waits for them, and re-layouts: 16.8 us -> 7.94 us
    dot_general x4 -> x8, matrix products: 22.6 us -> 30.8 us  [expert(): jnp.dot(expert_hidden(rows, weight_gate, weight_up), weight_down, preferr...]
    slice x8 -> x4, local copies, waits for them, and re-layouts: 10.8 us -> 4.16 us  [the longest x3 3.08 us: dense_per_device(): from_far = swapped(pairs[at - 1][rows_exp:], 'tp', 2)]
    concatenate x3 -> x4, local copies, waits for them, and re-layouts: 0.11 us -> 5.69 us  [dense_per_device(): lane = jnp.concatenate([held, swapped(held, 'tp', 2)], axis=0)]
    ppermute x6, starting transfers between devices: 4.59 us -> 9.61 us  [turned(): return lax.ppermute(x, axis, [(i, (i + by) % size) for i in range(size)])]
    dot_general x3 -> x6, matrix products: 4.53 us -> 8.6 us  [expert_hidden(): up_val = jnp.dot(rows, weight_up, preferred_element_type=jnp.float32)]
  transfers between devices with their start and end apart: 32 -> 28, of which waited for: 7 -> 10; matrix products, arithmetic and copies ran while one was open for 37% -> 40% of each run, Pallas kernels for 0% -> 0%
where the time goes in v2:
time: 215 us; the launch traced here: 214 us
  waiting for transfers between devices  92.8 us (43%)
  matrix products  60.5 us (28%)
  starting transfers between devices  26.6 us (12%)
  local copies, waits for them, and re-layouts  20.2 us (9%)
  other arithmetic  12.8 us (6%)
    ppermute x21, waiting for transfers between devices, swapped(): lax.ppermute(x, axis, [(i, i ^ mask) for i in range(lax.axis_size(axis))])  49.8 us
    ppermute x6, waiting for transfers between devices, turned(): return lax.ppermute(x, axis, [(i, (i + by) % size) for i in range(size)])  43 us
    dot_general x8, matrix products, expert(): jnp.dot(expert_hidden(rows, weight_gate, weight_up), weight_down, preferr...  30.8 us
    dot_general x6, matrix products, dense_per_device(): jnp.dot(lax.dynamic_slice_in_dim(gated_rows, first, piece.shape[0], axis=...  17.2 us
    ppermute x21, starting transfers between devices, swapped(): lax.ppermute(x, axis, [(i, i ^ mask) for i in range(lax.axis_size(axis))])  14.9 us
    ppermute x6, starting transfers between devices, turned(): return lax.ppermute(x, axis, [(i, (i + by) % size) for i in range(size)])  9.61 us
    dot_general x6, matrix products, expert_hidden(): up_val = jnp.dot(rows, weight_up, preferred_element_type=jnp.float32)  8.6 us
    unnamed x40, local copies, waits for them, and re-layouts  7.94 us
  transfers between devices with their start and end apart: 28, of which 10 were waited for; matrix products, arithmetic and copies ran while one was open for 40% of the time, Pallas kernels for 0%

profile of v2, /device:TPU:0, one launch (start us, length us, event | category | flops | bytes accessed | tf_op | source)
XLA Modules:
  0.0 214.0 jit_solution(964702174796733432)
XLA Ops:
  4.1 3.1 %collective-permute-start.6 = (bf16[128,2048]{1,0:T(8,128)(2,1)}, bf16[128,2048]{1,0:T(8,128)(2,1)}, u32[]{:S(2)}, u32[]{:S(2)}) collective-permute-start(bf16[128,2048]{1,0:T(8,128)(2,1)} %fusion.8), channel_id=1, source_target_pairs={{0,4},{4,8},{8,12},{12,0},{1,5},{5,9},{9,13},{13,1},{2,6},{6,10},{... | collective-permute-start | bytes 1572872 | tf_op jit(solution)/shard_map/ppermute | solution.py:107
  7.1 2.4 %constant_dynamic-slice_fusion = bf16[256,2048]{1,0:T(8,128)(2,1)} fusion(bf16[512,2048]{1,0:T(8,128)(2,1)} %param.16, s32[]{:T(128)S(6)} %select_n.56), kind=kLoop, calls=%fused_computation.124 | loop fusion | bytes 2097156 | tf_op jit(solution)/shard_map/dynamic_slice | solution.py:115
  11.5 2.1 collective-permute-start
  13.8 7.6 %collective-permute-done.6 = bf16[128,2048]{1,0:T(8,128)(2,1)} collective-permute-done((bf16[128,2048]{1,0:T(8,128)(2,1)}, bf16[128,2048]{1,0:T(8,128)(2,1)}, u32[]{:S(2)}, u32[]{:S(2)}) %collective-permute-start.6) | collective-permute-done | bytes 524320 | tf_op jit(solution)/shard_map/ppermute | solution.py:107
  24.1 22.5 %collective-permute-done.15 = bf16[128,2048]{1,0:T(8,128)(2,1)S(1)} collective-permute-done((bf16[128,2048]{1,0:T(8,128)(2,1)}, bf16[128,2048]{1,0:T(8,128)(2,1)S(1)}, u32[]{:S(2)}, u32[]{:S(2)}) %collective-permute-start.15) | collective-permute-done | bytes 524320 | tf_op jit(solution)/shard_map/ppermute | solution.py:102
  46.7 2.4 %multiply_convert_fusion = bf16[256,2048]{1,0:T(8,128)(2,1)S(1)} fusion(bf16[256,2048]{1,0:T(8,128)(2,1)S(1)} %multiply_convert_fusion.1, bf16[256,2048]{1,0:T(8,128)(2,1)} %param.14, bf16[2,2048]{1,0:T(2,128)(2,1)S(1)} %collective-permute-done, f32[2048]{0:T(1024)S(1)} %bitcast.111, f32[2048]{0:T(1024)S(1)} %bitcast.112, f32[2048]{0:T(1024)S(1)} %bitcast.110), kind=kLoop, calls=%fused_computation.14 | loop fusion | flops 8912896 | bytes 3178496 | tf_op jit(solution)/shard_map/convert_element_type | solution.py:167
  58.9 3.8 %convolution_convert_fusion.3 = bf16[256,2048]{1,0:T(8,128)(2,1)} fusion(bf16[1,256,2048]{2,1,0:T(8,128)(2,1)S(1)} %copy-done, f32[256,256]{1,0:T(8,128)S(1)} %fusion.35, bf16[256,2048]{1,0:T(8,128)(2,1)} %copy-done.13, bf16[1,2048,256]{2,1,0:T(8,128)(2,1)} %param.21), kind=kOutput, calls=%fused_computation.9 | convolution fusion | flops 537788416 | bytes 4456448 | tf_op jit(solution)/shard_map/dot_general | solution.py:183
  62.7 2.8 %collective-permute-done.13 = bf16[128,2048]{1,0:T(8,128)(2,1)} collective-permute-done((bf16[128,2048]{1,0:T(8,128)(2,1)}, bf16[128,2048]{1,0:T(8,128)(2,1)}, u32[]{:S(2)}, u32[]{:S(2)}) %collective-permute-start.13) | collective-permute-done | bytes 524320 | tf_op jit(solution)/shard_map/ppermute | solution.py:102
  71.0 3.0 %fusion.110 = f32[256,2048]{1,0:T(8,128)} fusion(bf16[256,2048]{1,0:T(8,128)(2,1)} %collective-permute-done.2, bf16[256,2048]{1,0:T(8,128)(2,1)S(1)} %multiply_convert_fusion, s32[]{:T(128)S(6)} %select_n.55), kind=kOutput, calls=%fused_computation.107 | convolution fusion | flops 268435456 | bytes 3276804 | tf_op jit(solution)/shard_map/dot_general | solution.py:170
  75.0 4.2 %add_convert_fusion.3 = bf16[256,2048]{1,0:T(8,128)(2,1)} fusion(bf16[256,2048]{1,0:T(8,128)(2,1)} %collective-permute-done.17, bf16[1,256,2048]{2,1,0:T(8,128)(2,1)S(1)} %copy-done, f32[256,256]{1,0:T(8,128)} %fusion.37, bf16[256,2048]{1,0:T(8,128)(2,1)} %copy-done.6, bf16[1,2048,256]{2,1,0:T(8,128)(2,1)} %param.21), kind=kOutput, calls=%fused_computation.13 | convolution fusion | flops 538836992 | bytes 5505024 | tf_op jit(solution)/shard_map/dot_general | solution.py:183
  79.2 2.5 %fusion.33 = f32[256,256]{1,0:T(8,128)} fusion(bf16[256,2048]{1,0:T(8,128)(2,1)} %collective-permute-done.14, bf16[1,2048,256]{2,1,0:T(8,128)(2,1)S(1)} %copy-done.1), kind=kOutput, calls=%fused_computation.43 | convolution fusion | flops 268435456 | bytes 2359296 | tf_op jit(solution)/shard_map/dot_general | solution.py:31
  81.6 3.6 %convolution_convert_fusion.2 = bf16[256,2048]{1,0:T(8,128)(2,1)} fusion(bf16[1,256,2048]{2,1,0:T(8,128)(2,1)S(1)} %copy-done, f32[256,256]{1,0:T(8,128)} %fusion.33, bf16[256,2048]{1,0:T(8,128)(2,1)} %collective-permute-done.14, bf16[1,2048,256]{2,1,0:T(8,128)(2,1)S(1)} %copy-done.4), kind=kOutput, calls=%fused_computation.8 | convolution fusion | flops 537788416 | bytes 4456448 | tf_op jit(solution)/shard_map/dot_general | solution.py:183
  90.0 5.8 %collective-permute-done.11 = bf16[128,2048]{1,0:T(8,128)(2,1)} collective-permute-done((bf16[128,2048]{1,0:T(8,128)(2,1)}, bf16[128,2048]{1,0:T(8,128)(2,1)}, u32[]{:S(2)}, u32[]{:S(2)}) %collective-permute-start.11) | collective-permute-done | bytes 524320 | tf_op jit(solution)/shard_map/ppermute | solution.py:102
  101.1 5.3 %collective-permute-done.19 = bf16[128,2048]{1,0:T(8,128)(2,1)S(1)} collective-permute-done((bf16[128,2048]{1,0:T(8,128)(2,1)S(1)}, bf16[128,2048]{1,0:T(8,128)(2,1)S(1)}, u32[]{:S(2)}, u32[]{:S(2)}) %collective-permute-start.19) | collective-permute-done | bytes 524320 | tf_op jit(solution)/shard_map/ppermute | solution.py:102
  107.3 3.8 %add_convert_fusion.2 = bf16[256,2048]{1,0:T(8,128)(2,1)} fusion(bf16[256,2048]{1,0:T(8,128)(2,1)} %collective-permute-done.18, bf16[1,256,2048]{2,1,0:T(8,128)(2,1)S(1)} %copy-done, f32[256,256]{1,0:T(8,128)S(1)} %fusion.39, bf16[256,2048]{1,0:T(8,128)(2,1)} %constant_dynamic-update-slice_fusion.4, bf16[1,2048,256]{2,1,0:T(8,128)(2,1)S(1)} %copy-done.4), kind=kOutput, calls=%fused_computation.12 | convolution fusion | flops 538836992 | bytes 5505024 | tf_op jit(solution)/shard_map/dot_general | solution.py:183
  116.3 3.5 %convolution_convert_fusion.1 = bf16[256,2048]{1,0:T(8,128)(2,1)} fusion(bf16[256,2048]{1,0:T(8,128)(2,1)} %collective-permute-done.12, bf16[1,256,2048]{2,1,0:T(8,128)(2,1)S(1)} %copy-done, bf16[1,2048,256]{2,1,0:T(8,128)(2,1)S(1)} %copy-done.1, f32[256,256]{1,0:T(8,128)S(1)} %fusion.47), kind=kOutput, calls=%fused_computation.7 | convolution fusion | flops 537788416 | bytes 4456448 | tf_op jit(solution)/shard_map/dot_general | solution.py:183
  121.8 2.4 %fusion.41 = f32[256,256]{1,0:T(8,128)} fusion(bf16[256,2048]{1,0:T(8,128)(2,1)} %constant_dynamic-update-slice_fusion.2, bf16[1,2048,256]{2,1,0:T(8,128)(2,1)S(1)} %copy-done.1), kind=kOutput, calls=%fused_computation.51 | convolution fusion | flops 268435456 | bytes 2359296 | tf_op jit(solution)/shard_map/dot_general | solution.py:31
  124.4 3.3 %collective-permute-done.21 = bf16[128,2048]{1,0:T(8,128)(2,1)} collective-permute-done((bf16[128,2048]{1,0:T(8,128)(2,1)}, bf16[128,2048]{1,0:T(8,128)(2,1)}, u32[]{:S(2)}, u32[]{:S(2)}) %collective-permute-start.21) | collective-permute-done | bytes 524320 | tf_op jit(solution)/shard_map/ppermute | solution.py:102
  129.7 4.0 %add_convert_fusion.1 = bf16[256,2048]{1,0:T(8,128)(2,1)} fusion(bf16[256,2048]{1,0:T(8,128)(2,1)} %collective-permute-done.20, bf16[1,256,2048]{2,1,0:T(8,128)(2,1)S(1)} %copy-done, f32[256,256]{1,0:T(8,128)} %fusion.41, bf16[256,2048]{1,0:T(8,128)(2,1)} %constant_dynamic-update-slice_fusion.2, bf16[1,2048,256]{2,1,0:T(8,128)(2,1)S(1)} %copy-done.4), kind=kOutput, calls=%fused_computation.11 | convolution fusion | flops 538836992 | bytes 5505024 | tf_op jit(solution)/shard_map/dot_general | solution.py:183
  133.6 2.4 %fusion.45 = f32[256,256]{1,0:T(8,128)} fusion(bf16[256,2048]{1,0:T(8,128)(2,1)} %collective-permute-done.9, bf16[1,2048,256]{2,1,0:T(8,128)(2,1)S(1)} %copy-done.4), kind=kOutput, calls=%fused_computation.55 | convolution fusion | flops 268435456 | bytes 2359296 | tf_op jit(solution)/shard_map/dot_general | solution.py:30
  136.0 3.6 %convolution_convert_fusion = bf16[256,2048]{1,0:T(8,128)(2,1)} fusion(bf16[256,2048]{1,0:T(8,128)(2,1)} %collective-permute-done.9, bf16[1,256,2048]{2,1,0:T(8,128)(2,1)S(1)} %copy-done, bf16[1,2048,256]{2,1,0:T(8,128)(2,1)S(1)} %copy-done.1, f32[256,256]{1,0:T(8,128)} %fusion.45), kind=kOutput, calls=%fused_computation.6 | convolution fusion | flops 537788416 | bytes 4456448 | tf_op jit(solution)/shard_map/dot_general | solution.py:183
  142.0 3.7 %fusion = f32[256,2048]{1,0:T(8,128)S(1)} fusion(f32[256,2048]{1,0:T(8,128)} %fusion.110, f32[256,2048]{1,0:T(8,128)} %fusion.72, bf16[512,2048]{1,0:T(8,128)(2,1)} %collective-permute-done.1, bf16[256,2048]{1,0:T(8,128)(2,1)} %copy-done.3, s32[]{:T(128)S(6)} %select_n.54), kind=kOutput, calls=%fused_computation.1 | convolution fusion | flops 537919488 | bytes 8650756 | tf_op jit(solution)/shard_map/dot_general | solution.py:170
  145.7 3.1 %fusion.107 = f32[256,2048]{1,0:T(8,128)} fusion(bf16[256,2048]{1,0:T(8,128)(2,1)} %collective-permute-done.4, bf16[256,2048]{1,0:T(8,128)(2,1)} %copy-done.3, s32[]{:T(128)S(6)} %select_n.58), kind=kOutput, calls=%fused_computation.104 | convolution fusion | flops 268435456 | bytes 3276804 | tf_op jit(solution)/shard_map/dot_general | solution.py:170
  148.9 2.2 %collective-permute-start.23 = (bf16[128,2048]{1,0:T(8,128)(2,1)}, bf16[128,2048]{1,0:T(8,128)(2,1)}, u32[]{:S(2)}, u32[]{:S(2)}) collective-permute-start(bf16[128,2048]{1,0:T(8,128)(2,1)} %add_convert_fusion.8), channel_id=1, source_target_pairs={{0,12},{4,0},{8,4},{12,8},{1,13},{5,1},{9,5},{13,9},{2,14},{6,2},{... | collective-permute-start | bytes 1572872 | tf_op jit(solution)/shard_map/ppermute | solution.py:107
  151.1 3.2 %collective-permute-done.25 = bf16[128,2048]{1,0:T(8,128)(2,1)S(1)} collective-permute-done((bf16[128,2048]{1,0:T(8,128)(2,1)S(1)}, bf16[128,2048]{1,0:T(8,128)(2,1)S(1)}, u32[]{:S(2)}, u32[]{:S(2)}) %collective-permute-start.25) | collective-permute-done | bytes 524320 | tf_op jit(solution)/shard_map/ppermute | solution.py:102
  154.3 2.7 %collective-permute-start.24 = (bf16[128,2048]{1,0:T(8,128)(2,1)}, bf16[128,2048]{1,0:T(8,128)(2,1)}, u32[]{:S(2)}, u32[]{:S(2)}) collective-permute-start(bf16[128,2048]{1,0:T(8,128)(2,1)} %add_convert_fusion.7), channel_id=1, source_target_pairs={{0,8},{4,12},{8,0},{12,4},{1,9},{5,13},{9,1},{13,5},{2,10},{6,14},... | collective-permute-start | bytes 1572872 | tf_op jit(solution)/shard_map/ppermute | solution.py:107
  157.9 4.2 %add_convert_fusion = bf16[256,2048]{1,0:T(8,128)(2,1)} fusion(bf16[256,2048]{1,0:T(8,128)(2,1)} %collective-permute-done.22, bf16[1,256,2048]{2,1,0:T(8,128)(2,1)S(1)} %copy-done, f32[256,256]{1,0:T(8,128)S(1)} %fusion.43, bf16[256,2048]{1,0:T(8,128)(2,1)} %constant_dynamic-update-slice_fusion, bf16[1,2048,256]{2,1,0:T(8,128)(2,1)} %param.21), kind=kOutput, calls=%fused_computation.10 | convolution fusion | flops 538836992 | bytes 5505024 | tf_op jit(solution)/shard_map/dot_general | solution.py:183
  163.8 33.6 %collective-permute-done.24 = bf16[128,2048]{1,0:T(8,128)(2,1)} collective-permute-done((bf16[128,2048]{1,0:T(8,128)(2,1)}, bf16[128,2048]{1,0:T(8,128)(2,1)}, u32[]{:S(2)}, u32[]{:S(2)}) %collective-permute-start.24) | collective-permute-done | bytes 524320 | tf_op jit(solution)/shard_map/ppermute | solution.py:107
  199.1 2.4 %fusion.1 = f32[256,2048]{1,0:T(8,128)S(1)} fusion(f32[256,2048]{1,0:T(8,128)} %fusion.107, f32[256,2048]{1,0:T(8,128)S(1)} %fusion, bf16[256,2048]{1,0:T(8,128)(2,1)} %collective-permute-done.3, bf16[256,2048]{1,0:T(8,128)(2,1)} %copy-done.3, s32[]{:T(128)S(6)} %select_n.57), kind=kOutput, calls=%fused_computation.4 | convolution fusion | flops 269484032 | bytes 7471108 | tf_op jit(solution)/shard_map/dot_general | solution.py:170
  201.6 2.8 %fusion.2 = bf16[256,2048]{1,0:T(8,128)(2,1)} fusion(f32[256,2048]{1,0:T(8,128)S(1)} %fusion.1, bf16[256,2048]{1,0:T(8,128)(2,1)} %collective-permute-done.5, bf16[256,2048]{1,0:T(8,128)(2,1)} %copy-done.3, s32[]{:T(128)S(6)} %select_n.59), kind=kOutput, calls=%fused_computation.5 | convolution fusion | flops 269484032 | bytes 4325380 | tf_op jit(solution)/shard_map/dot_general | solution.py:170
  204.4 6.9 %collective-permute-done.27 = bf16[128,2048]{1,0:T(8,128)(2,1)S(1)} collective-permute-done((bf16[128,2048]{1,0:T(8,128)(2,1)S(1)}, bf16[128,2048]{1,0:T(8,128)(2,1)S(1)}, u32[]{:S(2)}, u32[]{:S(2)}) %collective-permute-start.27) | collective-permute-done | bytes 524320 | tf_op jit(solution)/shard_map/ppermute | solution.py:102
  211.3 2.7 %add_convert_fusion.4 = bf16[128,2048]{1,0:T(8,128)(2,1)} fusion(bf16[128,2048]{1,0:T(8,128)(2,1)} %collective-permute-done.26, bf16[128,2048]{1,0:T(8,128)(2,1)} %collective-permute-done.24, bf16[128,2048]{1,0:T(8,128)(2,1)} %collective-permute-done.23, bf16[128,2048]{1,0:T(8,128)(2,1)S(1)} %collective-permute-done.27, f32[128]{0:T(128)S(1)} %get-tuple-element.33, ...), kind=kLoop, calls=%fused_computation.71 | loop fusion | flops 4194304 | bytes 3147776 | tf_op jit(solution)/shard_map/convert_element_type | solution.py:225
  (108 shorter events, 51.4 us)
Async XLA Ops:
  0.6 58.2 %copy-start = (bf16[1,256,2048]{2,1,0:T(8,128)(2,1)S(1)}, bf16[1,256,2048]{2,1,0:T(8,128)(2,1)}, u32[]{:S(2)}) copy-start(bf16[1,256,2048]{2,1,0:T(8,128)(2,1)} %param.23) | copy-start | bytes 3145732
  4.1 17.3 %collective-permute-start.6 = (bf16[128,2048]{1,0:T(8,128)(2,1)}, bf16[128,2048]{1,0:T(8,128)(2,1)}, u32[]{:S(2)}, u32[]{:S(2)}) collective-permute-start(bf16[128,2048]{1,0:T(8,128)(2,1)} %fusion.8), channel_id=1, source_target_pairs={{0,4},{4,8},{8,12},{12,0},{1,5},{5,9},{9,13},{13,1},{2,6},{6,10},{... | collective-permute-start | bytes 1572872 | tf_op jit(solution)/shard_map/ppermute | solution.py:107
  7.1 134.9 %collective-permute-start.1 = (bf16[512,2048]{1,0:T(8,128)(2,1)}, bf16[512,2048]{1,0:T(8,128)(2,1)}, u32[]{:S(2)}, u32[]{:S(2)}) collective-permute-start(bf16[512,2048]{1,0:T(8,128)(2,1)} %param.16), channel_id=1, source_target_pairs={{0,1},{1,0},{2,3},{3,2},{4,5},{5,4},{6,7},{7,6},{8,9},{9,8},{10,11... | collective-permute-start | bytes 6291464 | tf_op jit(solution)/shard_map/ppermute | solution.py:102
  9.5 59.9 %collective-permute-start.2 = (bf16[256,2048]{1,0:T(8,128)(2,1)}, bf16[256,2048]{1,0:T(8,128)(2,1)}, u32[]{:S(2)}, u32[]{:S(2)}) collective-permute-start(bf16[256,2048]{1,0:T(8,128)(2,1)} %constant_dynamic-slice_fusion), channel_id=1, source_target_pairs={{0,2},{1,3},{2,0},{3,1},{4,6},{5,7},{6,4},{7,5},{8,10},{9,11},{10,... | collective-permute-start | bytes 3145736 | tf_op jit(solution)/shard_map/ppermute | solution.py:102
  11.5 35.2 %collective-permute-start = (bf16[2,2048]{1,0:T(2,128)(2,1)S(1)}, bf16[2,2048]{1,0:T(2,128)(2,1)S(1)}, u32[]{:S(2)}, u32[]{:S(2)}) collective-permute-start(bf16[2,2048]{1,0:T(2,128)(2,1)S(1)} %slice.56), channel_id=1, source_target_pairs={{0,1},{1,2},{2,3},{3,4},{4,5},{5,6},{6,7},{7,8},{8,9},{9,10},{10,1... | collective-permute-start | bytes 24584 | tf_op jit(solution)/shard_map/ppermute | solution.py:13
  21.4 25.2 %collective-permute-start.15 = (bf16[128,2048]{1,0:T(8,128)(2,1)}, bf16[128,2048]{1,0:T(8,128)(2,1)S(1)}, u32[]{:S(2)}, u32[]{:S(2)}) collective-permute-start(bf16[128,2048]{1,0:T(8,128)(2,1)} %collective-permute-done.6), channel_id=1, source_target_pairs={{0,2},{1,3},{2,0},{3,1},{4,6},{5,7},{6,4},{7,5},{8,10},{9,11},{10,... | collective-permute-start | bytes 1572872 | tf_op jit(solution)/shard_map/ppermute | solution.py:102
  22.9 28.3 %collective-permute-start.7 = (bf16[128,2048]{1,0:T(8,128)(2,1)}, bf16[128,2048]{1,0:T(8,128)(2,1)}, u32[]{:S(2)}, u32[]{:S(2)}) collective-permute-start(bf16[128,2048]{1,0:T(8,128)(2,1)} %collective-permute-done.6), channel_id=1, source_target_pairs={{0,4},{4,8},{8,12},{12,0},{1,5},{5,9},{9,13},{13,1},{2,6},{6,10},{... | collective-permute-start | bytes 1572872 | tf_op jit(solution)/shard_map/ppermute | solution.py:107
  24.1 25.0 %copy-start.2 = (bf16[512,2048]{1,0:T(8,128)(2,1)S(1)}, bf16[512,2048]{1,0:T(8,128)(2,1)}, u32[]{:S(2)}) copy-start(bf16[512,2048]{1,0:T(8,128)(2,1)} %param.16) | copy-start | bytes 6291460
  46.6 10.8 %collective-permute-start.16 = (bf16[256,2048]{1,0:T(8,128)(2,1)S(1)}, bf16[256,2048]{1,0:T(8,128)(2,1)S(1)}, u32[]{:S(2)}, u32[]{:S(2)}) collective-permute-start(bf16[256,2048]{1,0:T(8,128)(2,1)S(1)} %constant_dynamic-update-slice_fusion.6), channel_id=1, source_target_pairs={{0,1},{1,0},{2,3},{3,2},{4,5},{5,4},{6,7},{7,6},{8,9},{9,8},{10,11... | collective-permute-start | bytes 3145736 | tf_op jit(solution)/shard_map/ppermute | solution.py:102
  49.1 21.9 %copy-start.3 = (bf16[256,2048]{1,0:T(8,128)(2,1)}, bf16[256,2048]{1,0:T(8,128)(2,1)S(1)}, u32[]{:S(2)}) copy-start(bf16[256,2048]{1,0:T(8,128)(2,1)S(1)} %multiply_convert_fusion) | copy-start | bytes 3145732
  51.2 14.3 %collective-permute-start.13 = (bf16[128,2048]{1,0:T(8,128)(2,1)}, bf16[128,2048]{1,0:T(8,128)(2,1)}, u32[]{:S(2)}, u32[]{:S(2)}) collective-permute-start(bf16[128,2048]{1,0:T(8,128)(2,1)} %collective-permute-done.7), channel_id=1, source_target_pairs={{0,2},{1,3},{2,0},{3,1},{4,6},{5,7},{6,4},{7,5},{8,10},{9,11},{10,... | collective-permute-start | bytes 1572872 | tf_op jit(solution)/shard_map/ppermute | solution.py:102
  52.8 21.3 %collective-permute-start.10 = (bf16[128,2048]{1,0:T(8,128)(2,1)}, bf16[128,2048]{1,0:T(8,128)(2,1)}, u32[]{:S(2)}, u32[]{:S(2)}) collective-permute-start(bf16[128,2048]{1,0:T(8,128)(2,1)} %collective-permute-done.7), channel_id=1, source_target_pairs={{0,4},{4,8},{8,12},{12,0},{1,5},{5,9},{9,13},{13,1},{2,6},{6,10},{... | collective-permute-start | bytes 1572872 | tf_op jit(solution)/shard_map/ppermute | solution.py:107
  62.7 12.3 %collective-permute-start.17 = (bf16[256,2048]{1,0:T(8,128)(2,1)}, bf16[256,2048]{1,0:T(8,128)(2,1)}, u32[]{:S(2)}, u32[]{:S(2)}) collective-permute-start(bf16[256,2048]{1,0:T(8,128)(2,1)} %convolution_convert_fusion.3), channel_id=1, source_target_pairs={{0,1},{1,0},{2,3},{3,2},{4,5},{5,4},{6,7},{7,6},{8,9},{9,8},{10,11... | collective-permute-start | bytes 3145736 | tf_op jit(solution)/shard_map/ppermute | solution.py:102
  67.4 11.8 %collective-permute-start.14 = (bf16[256,2048]{1,0:T(8,128)(2,1)}, bf16[256,2048]{1,0:T(8,128)(2,1)}, u32[]{:S(2)}, u32[]{:S(2)}) collective-permute-start(bf16[256,2048]{1,0:T(8,128)(2,1)} %constant_dynamic-update-slice_fusion.4), channel_id=1, source_target_pairs={{0,1},{1,0},{2,3},{3,2},{4,5},{5,4},{6,7},{7,6},{8,9},{9,8},{10,11... | collective-permute-start | bytes 3145736 | tf_op jit(solution)/shard_map/ppermute | solution.py:102
  69.4 29.8 %collective-permute-start.8 = (bf16[128,2048]{1,0:T(8,128)(2,1)}, bf16[128,2048]{1,0:T(8,128)(2,1)}, u32[]{:S(2)}, u32[]{:S(2)}) collective-permute-start(bf16[128,2048]{1,0:T(8,128)(2,1)} %fusion.8), channel_id=1, source_target_pairs={{0,2},{1,3},{2,0},{3,1},{4,6},{5,7},{6,4},{7,5},{8,10},{9,11},{10,... | collective-permute-start | bytes 1572872 | tf_op jit(solution)/shard_map/ppermute | solution.py:102
  74.1 21.7 %collective-permute-start.11 = (bf16[128,2048]{1,0:T(8,128)(2,1)}, bf16[128,2048]{1,0:T(8,128)(2,1)}, u32[]{:S(2)}, u32[]{:S(2)}) collective-permute-start(bf16[128,2048]{1,0:T(8,128)(2,1)} %collective-permute-done.10), channel_id=1, source_target_pairs={{0,2},{1,3},{2,0},{3,1},{4,6},{5,7},{6,4},{7,5},{8,10},{9,11},{10,... | collective-permute-start | bytes 1572872 | tf_op jit(solution)/shard_map/ppermute | solution.py:102
  85.3 21.1 %copy-start.9 = (bf16[256,2048]{1,0:T(8,128)(2,1)S(1)}, bf16[256,2048]{1,0:T(8,128)(2,1)}, u32[]{:S(2)}) copy-start(bf16[256,2048]{1,0:T(8,128)(2,1)} %add_convert_fusion.3) | copy-start | bytes 3145732
  85.3 22.1 %collective-permute-start.18 = (bf16[256,2048]{1,0:T(8,128)(2,1)}, bf16[256,2048]{1,0:T(8,128)(2,1)}, u32[]{:S(2)}, u32[]{:S(2)}) collective-permute-start(bf16[256,2048]{1,0:T(8,128)(2,1)} %convolution_convert_fusion.2), channel_id=1, source_target_pairs={{0,1},{1,0},{2,3},{3,2},{4,5},{5,4},{6,7},{7,6},{8,9},{9,8},{10,11... | collective-permute-start | bytes 3145736 | tf_op jit(solution)/shard_map/ppermute | solution.py:102
  86.4 19.9 %collective-permute-start.19 = (bf16[128,2048]{1,0:T(8,128)(2,1)S(1)}, bf16[128,2048]{1,0:T(8,128)(2,1)S(1)}, u32[]{:S(2)}, u32[]{:S(2)}) collective-permute-start(bf16[128,2048]{1,0:T(8,128)(2,1)S(1)} %slice.49), channel_id=1, source_target_pairs={{0,2},{1,3},{2,0},{3,1},{4,6},{5,7},{6,4},{7,5},{8,10},{9,11},{10,... | collective-permute-start | bytes 1572872 | tf_op jit(solution)/shard_map/ppermute | solution.py:102
  95.8 28.4 %collective-permute-start.4 = (bf16[256,2048]{1,0:T(8,128)(2,1)}, bf16[256,2048]{1,0:T(8,128)(2,1)}, u32[]{:S(2)}, u32[]{:S(2)}) collective-permute-start(bf16[256,2048]{1,0:T(8,128)(2,1)} %collective-permute-done.2), channel_id=1, source_target_pairs={{0,16},{16,0},{1,17},{17,1},{2,18},{18,2},{3,19},{19,3},{4,20},{20... | collective-permute-start | bytes 3145736 | tf_op jit(solution)/shard_map/ppermute | solution.py:102
  99.2 12.0 %collective-permute-start.12 = (bf16[256,2048]{1,0:T(8,128)(2,1)}, bf16[256,2048]{1,0:T(8,128)(2,1)}, u32[]{:S(2)}, u32[]{:S(2)}) collective-permute-start(bf16[256,2048]{1,0:T(8,128)(2,1)} %constant_dynamic-update-slice_fusion.2), channel_id=1, source_target_pairs={{0,1},{1,0},{2,3},{3,2},{4,5},{5,4},{6,7},{7,6},{8,9},{9,8},{10,11... | collective-permute-start | bytes 3145736 | tf_op jit(solution)/shard_map/ppermute | solution.py:102
  106.4 27.3 %collective-permute-start.9 = (bf16[256,2048]{1,0:T(8,128)(2,1)}, bf16[256,2048]{1,0:T(8,128)(2,1)}, u32[]{:S(2)}, u32[]{:S(2)}) collective-permute-start(bf16[256,2048]{1,0:T(8,128)(2,1)} %constant_dynamic-update-slice_fusion), channel_id=1, source_target_pairs={{0,1},{1,0},{2,3},{3,2},{4,5},{5,4},{6,7},{7,6},{8,9},{9,8},{10,11... | collective-permute-start | bytes 3145736 | tf_op jit(solution)/shard_map/ppermute | solution.py:102
  113.0 14.7 %collective-permute-start.21 = (bf16[128,2048]{1,0:T(8,128)(2,1)}, bf16[128,2048]{1,0:T(8,128)(2,1)}, u32[]{:S(2)}, u32[]{:S(2)}) collective-permute-start(bf16[128,2048]{1,0:T(8,128)(2,1)} %slice.51), channel_id=1, source_target_pairs={{0,2},{1,3},{2,0},{3,1},{4,6},{5,7},{6,4},{7,5},{8,10},{9,11},{10,... | collective-permute-start | bytes 1572872 | tf_op jit(solution)/shard_map/ppermute | solution.py:102
  119.8 9.9 %collective-permute-start.20 = (bf16[256,2048]{1,0:T(8,128)(2,1)}, bf16[256,2048]{1,0:T(8,128)(2,1)}, u32[]{:S(2)}, u32[]{:S(2)}) collective-permute-start(bf16[256,2048]{1,0:T(8,128)(2,1)} %convolution_convert_fusion.1), channel_id=1, source_target_pairs={{0,1},{1,0},{2,3},{3,2},{4,5},{5,4},{6,7},{7,6},{8,9},{9,8},{10,11... | collective-permute-start | bytes 3145736 | tf_op jit(solution)/shard_map/ppermute | solution.py:102
  124.2 75.0 %collective-permute-start.3 = (bf16[256,2048]{1,0:T(8,128)(2,1)}, bf16[256,2048]{1,0:T(8,128)(2,1)}, u32[]{:S(2)}, u32[]{:S(2)}) collective-permute-start(bf16[256,2048]{1,0:T(8,128)(2,1)} %collective-permute-done.2), channel_id=1, source_target_pairs={{0,1},{1,0},{2,3},{3,2},{4,5},{5,4},{6,7},{7,6},{8,9},{9,8},{10,11... | collective-permute-start | bytes 3145736 | tf_op jit(solution)/shard_map/ppermute | solution.py:102
  127.7 73.9 %collective-permute-start.5 = (bf16[256,2048]{1,0:T(8,128)(2,1)}, bf16[256,2048]{1,0:T(8,128)(2,1)}, u32[]{:S(2)}, u32[]{:S(2)}) collective-permute-start(bf16[256,2048]{1,0:T(8,128)(2,1)} %collective-permute-done.4), channel_id=1, source_target_pairs={{0,1},{1,0},{2,3},{3,2},{4,5},{5,4},{6,7},{7,6},{8,9},{9,8},{10,11... | collective-permute-start | bytes 3145736 | tf_op jit(solution)/shard_map/ppermute | solution.py:102
  139.6 18.3 %collective-permute-start.22 = (bf16[256,2048]{1,0:T(8,128)(2,1)}, bf16[256,2048]{1,0:T(8,128)(2,1)}, u32[]{:S(2)}, u32[]{:S(2)}) collective-permute-start(bf16[256,2048]{1,0:T(8,128)(2,1)} %convolution_convert_fusion), channel_id=1, source_target_pairs={{0,1},{1,0},{2,3},{3,2},{4,5},{5,4},{6,7},{7,6},{8,9},{9,8},{10,11... | collective-permute-start | bytes 3145736 | tf_op jit(solution)/shard_map/ppermute | solution.py:102
  140.2 14.1 %collective-permute-start.25 = (bf16[128,2048]{1,0:T(8,128)(2,1)S(1)}, bf16[128,2048]{1,0:T(8,128)(2,1)S(1)}, u32[]{:S(2)}, u32[]{:S(2)}) collective-permute-start(bf16[128,2048]{1,0:T(8,128)(2,1)S(1)} %slice.53), channel_id=1, source_target_pairs={{0,2},{1,3},{2,0},{3,1},{4,6},{5,7},{6,4},{7,5},{8,10},{9,11},{10,... | collective-permute-start | bytes 1572872 | tf_op jit(solution)/shard_map/ppermute | solution.py:102
  148.9 15.0 %collective-permute-start.23 = (bf16[128,2048]{1,0:T(8,128)(2,1)}, bf16[128,2048]{1,0:T(8,128)(2,1)}, u32[]{:S(2)}, u32[]{:S(2)}) collective-permute-start(bf16[128,2048]{1,0:T(8,128)(2,1)} %add_convert_fusion.8), channel_id=1, source_target_pairs={{0,12},{4,0},{8,4},{12,8},{1,13},{5,1},{9,5},{13,9},{2,14},{6,2},{... | collective-permute-start | bytes 1572872 | tf_op jit(solution)/shard_map/ppermute | solution.py:107
  154.3 43.2 %collective-permute-start.24 = (bf16[128,2048]{1,0:T(8,128)(2,1)}, bf16[128,2048]{1,0:T(8,128)(2,1)}, u32[]{:S(2)}, u32[]{:S(2)}) collective-permute-start(bf16[128,2048]{1,0:T(8,128)(2,1)} %add_convert_fusion.7), channel_id=1, source_target_pairs={{0,8},{4,12},{8,0},{12,4},{1,9},{5,13},{9,1},{13,5},{2,10},{6,14},... | collective-permute-start | bytes 1572872 | tf_op jit(solution)/shard_map/ppermute | solution.py:107
  157.9 46.5 %collective-permute-start.26 = (bf16[128,2048]{1,0:T(8,128)(2,1)}, bf16[128,2048]{1,0:T(8,128)(2,1)}, u32[]{:S(2)}, u32[]{:S(2)}) collective-permute-start(bf16[128,2048]{1,0:T(8,128)(2,1)} %add_convert_fusion.6), channel_id=1, source_target_pairs={{0,4},{4,8},{8,12},{12,0},{1,5},{5,9},{9,13},{13,1},{2,6},{6,10},{... | collective-permute-start | bytes 1572872 | tf_op jit(solution)/shard_map/ppermute | solution.py:107
  198.5 12.8 %collective-permute-start.27 = (bf16[128,2048]{1,0:T(8,128)(2,1)S(1)}, bf16[128,2048]{1,0:T(8,128)(2,1)S(1)}, u32[]{:S(2)}, u32[]{:S(2)}) collective-permute-start(bf16[128,2048]{1,0:T(8,128)(2,1)S(1)} %slice.55), channel_id=1, source_target_pairs={{0,2},{1,3},{2,0},{3,1},{4,6},{5,7},{6,4},{7,5},{8,10},{9,11},{10,... | collective-permute-start | bytes 1572872 | tf_op jit(solution)/shard_map/ppermute | solution.py:102
  (14 other events, 96.4 us)

commit v3 on v2

--- a/solution.py
+++ b/solution.py
@@ -107,12 +107,14 @@
     return lax.ppermute(x, axis, [(i, (i + by) % size) for i in range(size)])
 
 
-def gathered_pieces(w_out):
+def gathered_pieces(w_out, helds):
     me = lax.axis_index("tp")
     grp = lax.axis_index("grp")
     rows = w_out.shape[0]
     half = rows // 2
     mine = lax.dynamic_slice_in_dim(w_out, grp * half, half, axis=0)
+    if len(helds) > 2:
+        mine, helds[2] = lax.optimization_barrier((mine, helds[2]))
     far_mine = swapped(mine, "tp", 2)
     far_other = swapped(far_mine, "grp", 1)
     near = swapped(w_out, "tp", 1)
@@ -145,13 +147,16 @@
     n_ep = lax.axis_size("ep")
     my_ep = lax.axis_index("ep")
     rows_exp = route_b.shape[0]
-    pieces = gathered_pieces(w_out)
     tokens_f = tokens_b.astype(jnp.float32)
     normed = (
         tokens_f
         * lax.rsqrt(jnp.mean(tokens_f * tokens_f, axis=-1, keepdims=True) + 1e-06)
         * norm_gain
     ).astype(jnp.bfloat16)
+    helds = [normed]
+    for back in range(1, n_ep):
+        helds.append(turned(helds[-1], "ep", 1))
+    pieces = gathered_pieces(w_out, helds)
     shares = route_weights / jnp.sum(route_weights, axis=-1, keepdims=True)
 
     rows_mix = conv_x.shape[0]
@@ -186,19 +191,14 @@
             preferred_element_type=jnp.float32,
         )
 
-    helds = [normed]
-    for back in range(1, n_ep):
-        helds.append(turned(helds[-1], "ep", 1))
     order = [*range(1, n_ep), 0]
-    if n_ep > 2:
-        helds[0], helds[2] = lax.optimization_barrier((helds[0], helds[2]))
     pairs, sums, backs = [], [], []
     for at, back in enumerate(order):
         held = helds[back]
         lane = jnp.concatenate([held, swapped(held, "tp", 2)], axis=0)
         near = swapped(lane, "tp", 1)
         if at >= 1:
-            near, pairs[at - 1] = lax.optimization_barrier((near, pairs[at - 1]))
+            near, pairs[at - 1], *backs = lax.optimization_barrier((near, pairs[at - 1], *backs))
             from_far = swapped(pairs[at - 1][rows_exp:], "tp", 2)
             sums.append(
                 (

time: 215 us -> 228 us (1.060)
  waiting for transfers between devices: 92.8 us -> 105 us
  matrix products: 60.5 us -> 64.6 us
  local copies, waits for them, and re-layouts: 20.2 us -> 16.8 us
  other arithmetic: 12.8 us -> 16 us
  starting transfers between devices: 26.6 us -> 23.8 us
    ppermute x6, waiting for transfers between devices: 43 us -> 61 us  [turned(): return lax.ppermute(x, axis, [(i, (i + by) % size) for i in range(size)])]
    ppermute x21, waiting for transfers between devices: 49.8 us -> 43.7 us  [swapped(): lax.ppermute(x, axis, [(i, i ^ mask) for i in range(lax.axis_size(axis))])]
    concatenate x0 -> x1, other arithmetic: none -> 2.31 us  [dense_per_device(): lane = jnp.concatenate([held, swapped(held, 'tp', 2)], axis=0)]
    unnamed x40 -> x31, local copies, waits for them, and re-layouts: 7.94 us -> 5.74 us
    concatenate x4 -> x3, local copies, waits for them, and re-layouts: 5.69 us -> 4.63 us  [dense_per_device(): lane = jnp.concatenate([held, swapped(held, 'tp', 2)], axis=0)]
  transfers between devices with their start and end apart: 28 -> 28, of which waited for: 10 -> 12; matrix products, arithmetic and copies ran while one was open for 40% -> 40% of each run, Pallas kernels for 0% -> 0%
where the time goes in v3:
time: 228 us; the launch traced here: 227 us
  waiting for transfers between devices  105 us (46%)
  matrix products  64.6 us (28%)
  starting transfers between devices  23.8 us (10%)
  local copies, waits for them, and re-layouts  16.8 us (7%)
  other arithmetic  16 us (7%)
    ppermute x6, waiting for transfers between devices, turned(): return lax.ppermute(x, axis, [(i, (i + by) % size) for i in range(size)])  61 us
    ppermute x21, waiting for transfers between devices, swapped(): lax.ppermute(x, axis, [(i, i ^ mask) for i in range(lax.axis_size(axis))])  43.7 us
    dot_general x8, matrix products, expert(): jnp.dot(expert_hidden(rows, weight_gate, weight_up), weight_down, preferr...  31.1 us
    dot_general x6, matrix products, dense_per_device(): jnp.dot(lax.dynamic_slice_in_dim(gated_rows, first, piece.shape[0], axis=...  19.2 us
    ppermute x21, starting transfers between devices, swapped(): lax.ppermute(x, axis, [(i, i ^ mask) for i in range(lax.axis_size(axis))])  14.8 us
    dot_general x6, matrix products, expert_hidden(): up_val = jnp.dot(rows, weight_up, preferred_element_type=jnp.float32)  10.7 us
    ppermute x6, starting transfers between devices, turned(): return lax.ppermute(x, axis, [(i, (i + by) % size) for i in range(size)])  7.68 us
    unnamed x31, local copies, waits for them, and re-layouts  5.74 us
  transfers between devices with their start and end apart: 28, of which 12 were waited for; matrix products, arithmetic and copies ran while one was open for 40% of the time, Pallas kernels for 0%

profile of v3, /device:TPU:0, one launch (start us, length us, event | category | flops | bytes accessed | tf_op | source)
XLA Modules:
  0.0 226.9 jit_solution(13273777070077878025)
XLA Ops:
  4.1 3.1 %collective-permute-start.2 = (bf16[128,2048]{1,0:T(8,128)(2,1)}, bf16[128,2048]{1,0:T(8,128)(2,1)}, u32[]{:S(2)}, u32[]{:S(2)}) collective-permute-start(bf16[128,2048]{1,0:T(8,128)(2,1)} %fusion.8), channel_id=1, source_target_pairs={{0,4},{4,8},{8,12},{12,0},{1,5},{5,9},{9,13},{13,1},{2,6},{6,10},{... | collective-permute-start | bytes 1572872 | tf_op jit(solution)/shard_map/ppermute | solution.py:107
  12.9 8.5 %collective-permute-done.2 = bf16[128,2048]{1,0:T(8,128)(2,1)} collective-permute-done((bf16[128,2048]{1,0:T(8,128)(2,1)}, bf16[128,2048]{1,0:T(8,128)(2,1)}, u32[]{:S(2)}, u32[]{:S(2)}) %collective-permute-start.2) | collective-permute-done | bytes 524320 | tf_op jit(solution)/shard_map/ppermute | solution.py:107
  24.8 9.9 %collective-permute-done.15 = bf16[128,2048]{1,0:T(8,128)(2,1)S(1)} collective-permute-done((bf16[128,2048]{1,0:T(8,128)(2,1)}, bf16[128,2048]{1,0:T(8,128)(2,1)S(1)}, u32[]{:S(2)}, u32[]{:S(2)}) %collective-permute-start.15) | collective-permute-done | bytes 524320 | tf_op jit(solution)/shard_map/ppermute | solution.py:102
  35.5 2.3 %constant_dynamic-slice_fusion = bf16[256,2048]{1,0:T(8,128)(2,1)} fusion(bf16[512,2048]{1,0:T(8,128)(2,1)} %param.16, s32[]{:T(128)S(6)} %select_n.56), kind=kLoop, calls=%fused_computation.123 | loop fusion | bytes 2097156 | tf_op jit(solution)/shard_map/dynamic_slice | solution.py:115
  38.0 2.1 multiply_convert_fusion
  40.1 4.0 %fusion.72 = f32[256,2048]{1,0:T(8,128)} fusion(bf16[512,2048]{1,0:T(8,128)(2,1)} %param.16, bf16[256,2048]{1,0:T(8,128)(2,1)S(1)} %multiply_convert_fusion, s32[]{:T(128)S(6)} %select_n.53), kind=kOutput, calls=%fused_computation.94 | convolution fusion | flops 536870912 | bytes 4456452 | tf_op jit(solution)/shard_map/dot_general | solution.py:175
  44.1 10.3 %collective-permute-done.3 = bf16[128,2048]{1,0:T(8,128)(2,1)} collective-permute-done((bf16[128,2048]{1,0:T(8,128)(2,1)}, bf16[128,2048]{1,0:T(8,128)(2,1)}, u32[]{:S(2)}, u32[]{:S(2)}) %collective-permute-start.3) | collective-permute-done | bytes 524320 | tf_op jit(solution)/shard_map/ppermute | solution.py:107
  57.4 3.9 %convolution_convert_fusion.3 = bf16[256,2048]{1,0:T(8,128)(2,1)} fusion(bf16[1,256,2048]{2,1,0:T(8,128)(2,1)S(1)} %copy-done, f32[256,256]{1,0:T(8,128)S(1)} %fusion.35, bf16[256,2048]{1,0:T(8,128)(2,1)} %collective-permute-done.16, bf16[1,2048,256]{2,1,0:T(8,128)(2,1)} %param.21), kind=kOutput, calls=%fused_computation.9 | convolution fusion | flops 537788416 | bytes 4456448 | tf_op jit(solution)/shard_map/dot_general | solution.py:188
  63.1 5.1 %collective-permute-done.13 = bf16[128,2048]{1,0:T(8,128)(2,1)} collective-permute-done((bf16[128,2048]{1,0:T(8,128)(2,1)}, bf16[128,2048]{1,0:T(8,128)(2,1)}, u32[]{:S(2)}, u32[]{:S(2)}) %collective-permute-start.13) | collective-permute-done | bytes 524320 | tf_op jit(solution)/shard_map/ppermute | solution.py:102
  70.1 2.3 %fusion.43 = f32[256,256]{1,0:T(8,128)} fusion(bf16[1,2048,256]{2,1,0:T(8,128)(2,1)S(1)} %copy-done.1, bf16[128,2048]{1,0:T(8,128)(2,1)} %collective-permute-done.8, bf16[128,2048]{1,0:T(8,128)(2,1)} %fusion.8), kind=kOutput, calls=%fused_computation.54 | convolution fusion | flops 270532608 | bytes 2359296 | tf_op jit(solution)/shard_map/dot_general | solution.py:31
  72.5 2.3 %pad_maximum_fusion.1 = bf16[256,2048]{1,0:T(8,128)(2,1)} fusion(bf16[128,2048]{1,0:T(8,128)(2,1)} %collective-permute-done.8, bf16[128,2048]{1,0:T(8,128)(2,1)} %fusion.8), kind=kLoop, calls=%fused_computation.29 | loop fusion | flops 2097152 | bytes 2097152 | tf_op jit(solution)/shard_map/concatenate | solution.py:198
  77.7 11.2 %collective-permute-done.10 = bf16[128,2048]{1,0:T(8,128)(2,1)} collective-permute-done((bf16[128,2048]{1,0:T(8,128)(2,1)}, bf16[128,2048]{1,0:T(8,128)(2,1)}, u32[]{:S(2)}, u32[]{:S(2)}) %collective-permute-start.10) | collective-permute-done | bytes 524320 | tf_op jit(solution)/shard_map/ppermute | solution.py:107
  90.2 4.1 %add_convert_fusion.3 = bf16[256,2048]{1,0:T(8,128)(2,1)} fusion(bf16[256,2048]{1,0:T(8,128)(2,1)} %collective-permute-done.17, bf16[1,256,2048]{2,1,0:T(8,128)(2,1)S(1)} %copy-done, f32[256,256]{1,0:T(8,128)S(1)} %fusion.37, bf16[256,2048]{1,0:T(8,128)(2,1)} %constant_dynamic-update-slice_fusion.4, bf16[1,2048,256]{2,1,0:T(8,128)(2,1)} %param.21), kind=kOutput, calls=%fused_computation.13 | convolution fusion | flops 538836992 | bytes 5505024 | tf_op jit(solution)/shard_map/dot_general | solution.py:188
  96.0 3.8 %convolution_convert_fusion.2 = bf16[256,2048]{1,0:T(8,128)(2,1)} fusion(bf16[1,256,2048]{2,1,0:T(8,128)(2,1)S(1)} %copy-done, f32[256,256]{1,0:T(8,128)S(1)} %fusion.33, bf16[256,2048]{1,0:T(8,128)(2,1)} %collective-permute-done.14, bf16[1,2048,256]{2,1,0:T(8,128)(2,1)} %param.21), kind=kOutput, calls=%fused_computation.8 | convolution fusion | flops 537788416 | bytes 4456448 | tf_op jit(solution)/shard_map/dot_general | solution.py:188
  103.6 8.7 %collective-permute-done.11 = bf16[128,2048]{1,0:T(8,128)(2,1)} collective-permute-done((bf16[128,2048]{1,0:T(8,128)(2,1)}, bf16[128,2048]{1,0:T(8,128)(2,1)}, u32[]{:S(2)}, u32[]{:S(2)}) %collective-permute-start.11) | collective-permute-done | bytes 524320 | tf_op jit(solution)/shard_map/ppermute | solution.py:102
  116.5 6.5 %collective-permute-done.19 = bf16[128,2048]{1,0:T(8,128)(2,1)S(1)} collective-permute-done((bf16[128,2048]{1,0:T(8,128)(2,1)S(1)}, bf16[128,2048]{1,0:T(8,128)(2,1)S(1)}, u32[]{:S(2)}, u32[]{:S(2)}) %collective-permute-start.19) | collective-permute-done | bytes 524320 | tf_op jit(solution)/shard_map/ppermute | solution.py:102
  125.3 4.2 %add_convert_fusion.2 = bf16[256,2048]{1,0:T(8,128)(2,1)} fusion(bf16[256,2048]{1,0:T(8,128)(2,1)} %collective-permute-done.18, bf16[1,256,2048]{2,1,0:T(8,128)(2,1)S(1)} %copy-done, f32[256,256]{1,0:T(8,128)S(1)} %fusion.39, bf16[256,2048]{1,0:T(8,128)(2,1)} %constant_dynamic-update-slice_fusion.2, bf16[1,2048,256]{2,1,0:T(8,128)(2,1)} %param.21), kind=kOutput, calls=%fused_computation.12 | convolution fusion | flops 538836992 | bytes 5505024 | tf_op jit(solution)/shard_map/dot_general | solution.py:188
  134.8 3.5 %convolution_convert_fusion.1 = bf16[256,2048]{1,0:T(8,128)(2,1)} fusion(bf16[256,2048]{1,0:T(8,128)(2,1)} %collective-permute-done.12, bf16[1,256,2048]{2,1,0:T(8,128)(2,1)S(1)} %copy-done, bf16[1,2048,256]{2,1,0:T(8,128)(2,1)S(1)} %copy-done.1, f32[256,256]{1,0:T(8,128)S(1)} %fusion.47), kind=kOutput, calls=%fused_computation.7 | convolution fusion | flops 537788416 | bytes 4456448 | tf_op jit(solution)/shard_map/dot_general | solution.py:188
  138.3 3.1 %fusion.110 = f32[256,2048]{1,0:T(8,128)} fusion(bf16[256,2048]{1,0:T(8,128)(2,1)} %collective-permute-done.4, bf16[256,2048]{1,0:T(8,128)(2,1)S(1)} %multiply_convert_fusion, s32[]{:T(128)S(6)} %select_n.55), kind=kOutput, calls=%fused_computation.108 | convolution fusion | flops 268435456 | bytes 3276804 | tf_op jit(solution)/shard_map/dot_general | solution.py:175
  144.8 3.3 %collective-permute-start.21 = (bf16[128,2048]{1,0:T(8,128)(2,1)}, bf16[128,2048]{1,0:T(8,128)(2,1)}, u32[]{:S(2)}, u32[]{:S(2)}) collective-permute-start(bf16[128,2048]{1,0:T(8,128)(2,1)} %add_convert_fusion.8), channel_id=1, source_target_pairs={{0,12},{4,0},{8,4},{12,8},{1,13},{5,1},{9,5},{13,9},{2,14},{6,2},{... | collective-permute-start | bytes 1572872 | tf_op jit(solution)/shard_map/ppermute | solution.py:107
  150.1 3.8 %add_convert_fusion.1 = bf16[256,2048]{1,0:T(8,128)(2,1)} fusion(bf16[256,2048]{1,0:T(8,128)(2,1)} %collective-permute-done.20, bf16[1,256,2048]{2,1,0:T(8,128)(2,1)S(1)} %copy-done, f32[256,256]{1,0:T(8,128)S(1)} %fusion.41, bf16[256,2048]{1,0:T(8,128)(2,1)} %constant_dynamic-update-slice_fusion, bf16[1,2048,256]{2,1,0:T(8,128)(2,1)S(1)} %copy-done.3), kind=kOutput, calls=%fused_computation.11 | convolution fusion | flops 538836992 | bytes 5505024 | tf_op jit(solution)/shard_map/dot_general | solution.py:188
  153.9 4.9 %collective-permute-done.21 = bf16[128,2048]{1,0:T(8,128)(2,1)} collective-permute-done((bf16[128,2048]{1,0:T(8,128)(2,1)}, bf16[128,2048]{1,0:T(8,128)(2,1)}, u32[]{:S(2)}, u32[]{:S(2)}) %collective-permute-start.21) | collective-permute-done | bytes 524320 | tf_op jit(solution)/shard_map/ppermute | solution.py:107
  160.5 3.6 %convolution_convert_fusion = bf16[256,2048]{1,0:T(8,128)(2,1)} fusion(bf16[256,2048]{1,0:T(8,128)(2,1)} %collective-permute-done.9, bf16[1,256,2048]{2,1,0:T(8,128)(2,1)S(1)} %copy-done, bf16[1,2048,256]{2,1,0:T(8,128)(2,1)S(1)} %copy-done.1, f32[256,256]{1,0:T(8,128)S(1)} %fusion.45), kind=kOutput, calls=%fused_computation.6 | convolution fusion | flops 537788416 | bytes 4456448 | tf_op jit(solution)/shard_map/dot_general | solution.py:188
  164.9 3.7 %fusion = f32[256,2048]{1,0:T(8,128)S(1)} fusion(f32[256,2048]{1,0:T(8,128)} %fusion.110, f32[256,2048]{1,0:T(8,128)} %fusion.72, bf16[512,2048]{1,0:T(8,128)(2,1)} %collective-permute-done.1, bf16[256,2048]{1,0:T(8,128)(2,1)} %copy-done.2, s32[]{:T(128)S(6)} %select_n.54), kind=kOutput, calls=%fused_computation.1 | convolution fusion | flops 537919488 | bytes 8650756 | tf_op jit(solution)/shard_map/dot_general | solution.py:175
  168.9 3.1 %fusion.107 = f32[256,2048]{1,0:T(8,128)} fusion(bf16[256,2048]{1,0:T(8,128)(2,1)} %collective-permute-done.6, bf16[256,2048]{1,0:T(8,128)(2,1)} %copy-done.2, s32[]{:T(128)S(6)} %select_n.58), kind=kOutput, calls=%fused_computation.105 | convolution fusion | flops 268435456 | bytes 3276804 | tf_op jit(solution)/shard_map/dot_general | solution.py:175
  173.4 5.3 %collective-permute-done.25 = bf16[128,2048]{1,0:T(8,128)(2,1)S(1)} collective-permute-done((bf16[128,2048]{1,0:T(8,128)(2,1)S(1)}, bf16[128,2048]{1,0:T(8,128)(2,1)S(1)}, u32[]{:S(2)}, u32[]{:S(2)}) %collective-permute-start.25) | collective-permute-done | bytes 524320 | tf_op jit(solution)/shard_map/ppermute | solution.py:102
  179.5 4.2 %add_convert_fusion = bf16[256,2048]{1,0:T(8,128)(2,1)} fusion(bf16[256,2048]{1,0:T(8,128)(2,1)} %collective-permute-done.23, bf16[1,256,2048]{2,1,0:T(8,128)(2,1)S(1)} %copy-done, f32[256,256]{1,0:T(8,128)S(1)} %copy-done.13, bf16[1,2048,256]{2,1,0:T(8,128)(2,1)} %param.21, bf16[128,2048]{1,0:T(8,128)(2,1)} %collective-permute-done.8, ...), kind=kOutput, calls=%fused_computation.10 | convolution fusion | flops 540934144 | bytes 5505024 | tf_op jit(solution)/shard_map/dot_general | solution.py:188
  183.7 26.1 %collective-permute-done.24 = bf16[128,2048]{1,0:T(8,128)(2,1)} collective-permute-done((bf16[128,2048]{1,0:T(8,128)(2,1)}, bf16[128,2048]{1,0:T(8,128)(2,1)}, u32[]{:S(2)}, u32[]{:S(2)}) %collective-permute-start.24) | collective-permute-done | bytes 524320 | tf_op jit(solution)/shard_map/ppermute | solution.py:107
  212.4 2.4 %fusion.1 = f32[256,2048]{1,0:T(8,128)S(1)} fusion(f32[256,2048]{1,0:T(8,128)} %fusion.107, f32[256,2048]{1,0:T(8,128)S(1)} %fusion, bf16[256,2048]{1,0:T(8,128)(2,1)} %collective-permute-done.5, bf16[256,2048]{1,0:T(8,128)(2,1)} %copy-done.2, s32[]{:T(128)S(6)} %select_n.57), kind=kOutput, calls=%fused_computation.4 | convolution fusion | flops 269484032 | bytes 7471108 | tf_op jit(solution)/shard_map/dot_general | solution.py:175
  214.8 2.8 %fusion.2 = bf16[256,2048]{1,0:T(8,128)(2,1)} fusion(f32[256,2048]{1,0:T(8,128)S(1)} %fusion.1, bf16[256,2048]{1,0:T(8,128)(2,1)} %collective-permute-done.7, bf16[256,2048]{1,0:T(8,128)(2,1)} %copy-done.2, s32[]{:T(128)S(6)} %select_n.59), kind=kOutput, calls=%fused_computation.5 | convolution fusion | flops 269484032 | bytes 4325380 | tf_op jit(solution)/shard_map/dot_general | solution.py:175
  217.6 6.6 %collective-permute-done.27 = bf16[128,2048]{1,0:T(8,128)(2,1)S(1)} collective-permute-done((bf16[128,2048]{1,0:T(8,128)(2,1)S(1)}, bf16[128,2048]{1,0:T(8,128)(2,1)S(1)}, u32[]{:S(2)}, u32[]{:S(2)}) %collective-permute-start.27) | collective-permute-done | bytes 524320 | tf_op jit(solution)/shard_map/ppermute | solution.py:102
  224.2 2.7 %add_convert_fusion.4 = bf16[128,2048]{1,0:T(8,128)(2,1)} fusion(bf16[128,2048]{1,0:T(8,128)(2,1)} %collective-permute-done.26, bf16[128,2048]{1,0:T(8,128)(2,1)} %collective-permute-done.24, bf16[128,2048]{1,0:T(8,128)(2,1)} %collective-permute-done.21, bf16[128,2048]{1,0:T(8,128)(2,1)S(1)} %collective-permute-done.27, f32[128]{0:T(128)S(1)} %get-tuple-element.35, ...), kind=kLoop, calls=%fused_computation.72 | loop fusion | flops 4194304 | bytes 3147776 | tf_op jit(solution)/shard_map/convert_element_type | solution.py:225
  (99 shorter events, 54.6 us)
Async XLA Ops:
  0.6 56.8 %copy-start = (bf16[1,256,2048]{2,1,0:T(8,128)(2,1)S(1)}, bf16[1,256,2048]{2,1,0:T(8,128)(2,1)}, u32[]{:S(2)}) copy-start(bf16[1,256,2048]{2,1,0:T(8,128)(2,1)} %param.23) | copy-start | bytes 3145732
  2.0 20.9 %copy-start.10 = (f32[3,2048]{1,0:T(4,128)S(1)}, f32[3,2048]{1,0:T(4,128)}, u32[]{:S(2)}) copy-start(f32[3,2048]{1,0:T(4,128)} %param.15) | copy-start | bytes 73732
  4.1 17.3 %collective-permute-start.2 = (bf16[128,2048]{1,0:T(8,128)(2,1)}, bf16[128,2048]{1,0:T(8,128)(2,1)}, u32[]{:S(2)}, u32[]{:S(2)}) collective-permute-start(bf16[128,2048]{1,0:T(8,128)(2,1)} %fusion.8), channel_id=1, source_target_pairs={{0,4},{4,8},{8,12},{12,0},{1,5},{5,9},{9,13},{13,1},{2,6},{6,10},{... | collective-permute-start | bytes 1572872 | tf_op jit(solution)/shard_map/ppermute | solution.py:107
  7.1 63.0 %collective-permute-start.8 = (bf16[128,2048]{1,0:T(8,128)(2,1)}, bf16[128,2048]{1,0:T(8,128)(2,1)}, u32[]{:S(2)}, u32[]{:S(2)}) collective-permute-start(bf16[128,2048]{1,0:T(8,128)(2,1)} %fusion.8), channel_id=1, source_target_pairs={{0,2},{1,3},{2,0},{3,1},{4,6},{5,7},{6,4},{7,5},{8,10},{9,11},{10,... | collective-permute-start | bytes 1572872 | tf_op jit(solution)/shard_map/ppermute | solution.py:102
  10.3 27.7 %collective-permute-start = (bf16[2,2048]{1,0:T(2,128)(2,1)S(1)}, bf16[2,2048]{1,0:T(2,128)(2,1)S(1)}, u32[]{:S(2)}, u32[]{:S(2)}) collective-permute-start(bf16[2,2048]{1,0:T(2,128)(2,1)S(1)} %slice.56), channel_id=1, source_target_pairs={{0,1},{1,2},{2,3},{3,4},{4,5},{5,6},{6,7},{7,8},{8,9},{9,10},{10,1... | collective-permute-start | bytes 24584 | tf_op jit(solution)/shard_map/ppermute | solution.py:13
  11.6 153.3 %collective-permute-start.1 = (bf16[512,2048]{1,0:T(8,128)(2,1)}, bf16[512,2048]{1,0:T(8,128)(2,1)}, u32[]{:S(2)}, u32[]{:S(2)}) collective-permute-start(bf16[512,2048]{1,0:T(8,128)(2,1)} %param.16), channel_id=1, source_target_pairs={{0,1},{1,0},{2,3},{3,2},{4,5},{5,4},{6,7},{7,6},{8,9},{9,8},{10,11... | collective-permute-start | bytes 6291464 | tf_op jit(solution)/shard_map/ppermute | solution.py:102
  21.4 13.3 %collective-permute-start.15 = (bf16[128,2048]{1,0:T(8,128)(2,1)}, bf16[128,2048]{1,0:T(8,128)(2,1)S(1)}, u32[]{:S(2)}, u32[]{:S(2)}) collective-permute-start(bf16[128,2048]{1,0:T(8,128)(2,1)} %collective-permute-done.2), channel_id=1, source_target_pairs={{0,2},{1,3},{2,0},{3,1},{4,6},{5,7},{6,4},{7,5},{8,10},{9,11},{10,... | collective-permute-start | bytes 1572872 | tf_op jit(solution)/shard_map/ppermute | solution.py:102
  35.5 20.2 %collective-permute-start.16 = (bf16[256,2048]{1,0:T(8,128)(2,1)}, bf16[256,2048]{1,0:T(8,128)(2,1)}, u32[]{:S(2)}, u32[]{:S(2)}) collective-permute-start(bf16[256,2048]{1,0:T(8,128)(2,1)} %constant_dynamic-update-slice_fusion.4), channel_id=1, source_target_pairs={{0,1},{1,0},{2,3},{3,2},{4,5},{5,4},{6,7},{7,6},{8,9},{9,8},{10,11... | collective-permute-start | bytes 3145736 | tf_op jit(solution)/shard_map/ppermute | solution.py:102
  37.9 16.5 %collective-permute-start.3 = (bf16[128,2048]{1,0:T(8,128)(2,1)}, bf16[128,2048]{1,0:T(8,128)(2,1)}, u32[]{:S(2)}, u32[]{:S(2)}) collective-permute-start(bf16[128,2048]{1,0:T(8,128)(2,1)} %collective-permute-done.2), channel_id=1, source_target_pairs={{0,4},{4,8},{8,12},{12,0},{1,5},{5,9},{9,13},{13,1},{2,6},{6,10},{... | collective-permute-start | bytes 1572872 | tf_op jit(solution)/shard_map/ppermute | solution.py:107
  40.1 98.2 %copy-start.2 = (bf16[256,2048]{1,0:T(8,128)(2,1)}, bf16[256,2048]{1,0:T(8,128)(2,1)S(1)}, u32[]{:S(2)}) copy-start(bf16[256,2048]{1,0:T(8,128)(2,1)S(1)} %multiply_convert_fusion) | copy-start | bytes 3145732
  54.4 13.8 %collective-permute-start.13 = (bf16[128,2048]{1,0:T(8,128)(2,1)}, bf16[128,2048]{1,0:T(8,128)(2,1)}, u32[]{:S(2)}, u32[]{:S(2)}) collective-permute-start(bf16[128,2048]{1,0:T(8,128)(2,1)} %collective-permute-done.3), channel_id=1, source_target_pairs={{0,2},{1,3},{2,0},{3,1},{4,6},{5,7},{6,4},{7,5},{8,10},{9,11},{10,... | collective-permute-start | bytes 1572872 | tf_op jit(solution)/shard_map/ppermute | solution.py:102
  61.2 28.9 %collective-permute-start.17 = (bf16[256,2048]{1,0:T(8,128)(2,1)}, bf16[256,2048]{1,0:T(8,128)(2,1)}, u32[]{:S(2)}, u32[]{:S(2)}) collective-permute-start(bf16[256,2048]{1,0:T(8,128)(2,1)} %convolution_convert_fusion.3), channel_id=1, source_target_pairs={{0,1},{1,0},{2,3},{3,2},{4,5},{5,4},{6,7},{7,6},{8,9},{9,8},{10,11... | collective-permute-start | bytes 3145736 | tf_op jit(solution)/shard_map/ppermute | solution.py:102
  70.1 24.2 %collective-permute-start.14 = (bf16[256,2048]{1,0:T(8,128)(2,1)}, bf16[256,2048]{1,0:T(8,128)(2,1)}, u32[]{:S(2)}, u32[]{:S(2)}) collective-permute-start(bf16[256,2048]{1,0:T(8,128)(2,1)} %constant_dynamic-update-slice_fusion.2), channel_id=1, source_target_pairs={{0,1},{1,0},{2,3},{3,2},{4,5},{5,4},{6,7},{7,6},{8,9},{9,8},{10,11... | collective-permute-start | bytes 3145736 | tf_op jit(solution)/shard_map/ppermute | solution.py:102
  72.5 16.5 %collective-permute-start.10 = (bf16[128,2048]{1,0:T(8,128)(2,1)}, bf16[128,2048]{1,0:T(8,128)(2,1)}, u32[]{:S(2)}, u32[]{:S(2)}) collective-permute-start(bf16[128,2048]{1,0:T(8,128)(2,1)} %collective-permute-done.3), channel_id=1, source_target_pairs={{0,4},{4,8},{8,12},{12,0},{1,5},{5,9},{9,13},{13,1},{2,6},{6,10},{... | collective-permute-start | bytes 1572872 | tf_op jit(solution)/shard_map/ppermute | solution.py:107
  74.8 41.2 %collective-permute-start.4 = (bf16[256,2048]{1,0:T(8,128)(2,1)}, bf16[256,2048]{1,0:T(8,128)(2,1)}, u32[]{:S(2)}, u32[]{:S(2)}) collective-permute-start(bf16[256,2048]{1,0:T(8,128)(2,1)} %constant_dynamic-slice_fusion), channel_id=1, source_target_pairs={{0,2},{1,3},{2,0},{3,1},{4,6},{5,7},{6,4},{7,5},{8,10},{9,11},{10,... | collective-permute-start | bytes 3145736 | tf_op jit(solution)/shard_map/ppermute | solution.py:102
  88.9 23.4 %collective-permute-start.11 = (bf16[128,2048]{1,0:T(8,128)(2,1)}, bf16[128,2048]{1,0:T(8,128)(2,1)}, u32[]{:S(2)}, u32[]{:S(2)}) collective-permute-start(bf16[128,2048]{1,0:T(8,128)(2,1)} %collective-permute-done.10), channel_id=1, source_target_pairs={{0,2},{1,3},{2,0},{3,1},{4,6},{5,7},{6,4},{7,5},{8,10},{9,11},{10,... | collective-permute-start | bytes 1572872 | tf_op jit(solution)/shard_map/ppermute | solution.py:102
  99.8 25.4 %collective-permute-start.18 = (bf16[256,2048]{1,0:T(8,128)(2,1)}, bf16[256,2048]{1,0:T(8,128)(2,1)}, u32[]{:S(2)}, u32[]{:S(2)}) collective-permute-start(bf16[256,2048]{1,0:T(8,128)(2,1)} %convolution_convert_fusion.2), channel_id=1, source_target_pairs={{0,1},{1,0},{2,3},{3,2},{4,5},{5,4},{6,7},{7,6},{8,9},{9,8},{10,11... | collective-permute-start | bytes 3145736 | tf_op jit(solution)/shard_map/ppermute | solution.py:102
  100.9 23.4 %copy-start.7 = (bf16[256,2048]{1,0:T(8,128)(2,1)S(1)}, bf16[256,2048]{1,0:T(8,128)(2,1)}, u32[]{:S(2)}) copy-start(bf16[256,2048]{1,0:T(8,128)(2,1)} %add_convert_fusion.3) | copy-start | bytes 3145732
  100.9 22.1 %collective-permute-start.19 = (bf16[128,2048]{1,0:T(8,128)(2,1)S(1)}, bf16[128,2048]{1,0:T(8,128)(2,1)S(1)}, u32[]{:S(2)}, u32[]{:S(2)}) collective-permute-start(bf16[128,2048]{1,0:T(8,128)(2,1)S(1)} %slice.49), channel_id=1, source_target_pairs={{0,2},{1,3},{2,0},{3,1},{4,6},{5,7},{6,4},{7,5},{8,10},{9,11},{10,... | collective-permute-start | bytes 1572872 | tf_op jit(solution)/shard_map/ppermute | solution.py:102
  114.3 15.2 %collective-permute-start.12 = (bf16[256,2048]{1,0:T(8,128)(2,1)}, bf16[256,2048]{1,0:T(8,128)(2,1)}, u32[]{:S(2)}, u32[]{:S(2)}) collective-permute-start(bf16[256,2048]{1,0:T(8,128)(2,1)} %constant_dynamic-update-slice_fusion), channel_id=1, source_target_pairs={{0,1},{1,0},{2,3},{3,2},{4,5},{5,4},{6,7},{7,6},{8,9},{9,8},{10,11... | collective-permute-start | bytes 3145736 | tf_op jit(solution)/shard_map/ppermute | solution.py:102
  115.9 38.0 %collective-permute-start.9 = (bf16[256,2048]{1,0:T(8,128)(2,1)}, bf16[256,2048]{1,0:T(8,128)(2,1)}, u32[]{:S(2)}, u32[]{:S(2)}) collective-permute-start(bf16[256,2048]{1,0:T(8,128)(2,1)} %pad_maximum_fusion.1), channel_id=1, source_target_pairs={{0,1},{1,0},{2,3},{3,2},{4,5},{5,4},{6,7},{7,6},{8,9},{9,8},{10,11... | collective-permute-start | bytes 3145736 | tf_op jit(solution)/shard_map/ppermute | solution.py:102
  123.0 45.6 %collective-permute-start.6 = (bf16[256,2048]{1,0:T(8,128)(2,1)}, bf16[256,2048]{1,0:T(8,128)(2,1)}, u32[]{:S(2)}, u32[]{:S(2)}) collective-permute-start(bf16[256,2048]{1,0:T(8,128)(2,1)} %collective-permute-done.4), channel_id=1, source_target_pairs={{0,16},{16,0},{1,17},{17,1},{2,18},{18,2},{3,19},{19,3},{4,20},{20... | collective-permute-start | bytes 3145736 | tf_op jit(solution)/shard_map/ppermute | solution.py:102
  131.3 13.5 %collective-permute-start.22 = (bf16[128,2048]{1,0:T(8,128)(2,1)}, bf16[128,2048]{1,0:T(8,128)(2,1)}, u32[]{:S(2)}, u32[]{:S(2)}) collective-permute-start(bf16[128,2048]{1,0:T(8,128)(2,1)} %slice.51), channel_id=1, source_target_pairs={{0,2},{1,3},{2,0},{3,1},{4,6},{5,7},{6,4},{7,5},{8,10},{9,11},{10,... | collective-permute-start | bytes 1572872 | tf_op jit(solution)/shard_map/ppermute | solution.py:102
  138.3 11.8 %collective-permute-start.20 = (bf16[256,2048]{1,0:T(8,128)(2,1)}, bf16[256,2048]{1,0:T(8,128)(2,1)}, u32[]{:S(2)}, u32[]{:S(2)}) collective-permute-start(bf16[256,2048]{1,0:T(8,128)(2,1)} %convolution_convert_fusion.1), channel_id=1, source_target_pairs={{0,1},{1,0},{2,3},{3,2},{4,5},{5,4},{6,7},{7,6},{8,9},{9,8},{10,11... | collective-permute-start | bytes 3145736 | tf_op jit(solution)/shard_map/ppermute | solution.py:102
  144.8 14.0 %collective-permute-start.21 = (bf16[128,2048]{1,0:T(8,128)(2,1)}, bf16[128,2048]{1,0:T(8,128)(2,1)}, u32[]{:S(2)}, u32[]{:S(2)}) collective-permute-start(bf16[128,2048]{1,0:T(8,128)(2,1)} %add_convert_fusion.8), channel_id=1, source_target_pairs={{0,12},{4,0},{8,4},{12,8},{1,13},{5,1},{9,5},{13,9},{2,14},{6,2},{... | collective-permute-start | bytes 1572872 | tf_op jit(solution)/shard_map/ppermute | solution.py:107
  150.1 62.3 %collective-permute-start.5 = (bf16[256,2048]{1,0:T(8,128)(2,1)}, bf16[256,2048]{1,0:T(8,128)(2,1)}, u32[]{:S(2)}, u32[]{:S(2)}) collective-permute-start(bf16[256,2048]{1,0:T(8,128)(2,1)} %collective-permute-done.4), channel_id=1, source_target_pairs={{0,1},{1,0},{2,3},{3,2},{4,5},{5,4},{6,7},{7,6},{8,9},{9,8},{10,11... | collective-permute-start | bytes 3145736 | tf_op jit(solution)/shard_map/ppermute | solution.py:102
  164.1 15.4 %collective-permute-start.23 = (bf16[256,2048]{1,0:T(8,128)(2,1)}, bf16[256,2048]{1,0:T(8,128)(2,1)}, u32[]{:S(2)}, u32[]{:S(2)}) collective-permute-start(bf16[256,2048]{1,0:T(8,128)(2,1)} %convolution_convert_fusion), channel_id=1, source_target_pairs={{0,1},{1,0},{2,3},{3,2},{4,5},{5,4},{6,7},{7,6},{8,9},{9,8},{10,11... | collective-permute-start | bytes 3145736 | tf_op jit(solution)/shard_map/ppermute | solution.py:102
  164.2 14.4 %collective-permute-start.25 = (bf16[128,2048]{1,0:T(8,128)(2,1)S(1)}, bf16[128,2048]{1,0:T(8,128)(2,1)S(1)}, u32[]{:S(2)}, u32[]{:S(2)}) collective-permute-start(bf16[128,2048]{1,0:T(8,128)(2,1)S(1)} %slice.53), channel_id=1, source_target_pairs={{0,2},{1,3},{2,0},{3,1},{4,6},{5,7},{6,4},{7,5},{8,10},{9,11},{10,... | collective-permute-start | bytes 1572872 | tf_op jit(solution)/shard_map/ppermute | solution.py:102
  168.6 46.2 %collective-permute-start.7 = (bf16[256,2048]{1,0:T(8,128)(2,1)}, bf16[256,2048]{1,0:T(8,128)(2,1)}, u32[]{:S(2)}, u32[]{:S(2)}) collective-permute-start(bf16[256,2048]{1,0:T(8,128)(2,1)} %collective-permute-done.6), channel_id=1, source_target_pairs={{0,1},{1,0},{2,3},{3,2},{4,5},{5,4},{6,7},{7,6},{8,9},{9,8},{10,11... | collective-permute-start | bytes 3145736 | tf_op jit(solution)/shard_map/ppermute | solution.py:102
  172.0 37.8 %collective-permute-start.24 = (bf16[128,2048]{1,0:T(8,128)(2,1)}, bf16[128,2048]{1,0:T(8,128)(2,1)}, u32[]{:S(2)}, u32[]{:S(2)}) collective-permute-start(bf16[128,2048]{1,0:T(8,128)(2,1)} %add_convert_fusion.7), channel_id=1, source_target_pairs={{0,8},{4,12},{8,0},{12,4},{1,9},{5,13},{9,1},{13,5},{2,10},{6,14},... | collective-permute-start | bytes 1572872 | tf_op jit(solution)/shard_map/ppermute | solution.py:107
  179.5 38.1 %collective-permute-start.26 = (bf16[128,2048]{1,0:T(8,128)(2,1)}, bf16[128,2048]{1,0:T(8,128)(2,1)}, u32[]{:S(2)}, u32[]{:S(2)}) collective-permute-start(bf16[128,2048]{1,0:T(8,128)(2,1)} %add_convert_fusion.6), channel_id=1, source_target_pairs={{0,4},{4,8},{8,12},{12,0},{1,5},{5,9},{9,13},{13,1},{2,6},{6,10},{... | collective-permute-start | bytes 1572872 | tf_op jit(solution)/shard_map/ppermute | solution.py:107
  210.9 13.3 %collective-permute-start.27 = (bf16[128,2048]{1,0:T(8,128)(2,1)S(1)}, bf16[128,2048]{1,0:T(8,128)(2,1)S(1)}, u32[]{:S(2)}, u32[]{:S(2)}) collective-permute-start(bf16[128,2048]{1,0:T(8,128)(2,1)S(1)} %slice.55), channel_id=1, source_target_pairs={{0,2},{1,3},{2,0},{3,1},{4,6},{5,7},{6,4},{7,5},{8,10},{9,11},{10,... | collective-permute-start | bytes 1572872 | tf_op jit(solution)/shard_map/ppermute | solution.py:102
  (10 other events, 106.0 us)
